TPU v7x, 256 devices: a whole 4x4x8 slice. The times are simulated.
256 devices in a mesh: dp: 4 (over x), kv: 32 (over z, y), tp: 2 (over core).
Axes of the slice: x: 4, y: 4, z: 8, core: 2. Of those that a mesh axis runs over, the one named last changes fastest.
Arguments:
- tokens: bfloat16 [16, 2048], P('dp', 'kv'), may hold values from -700 to 700
- norm_gain: float32 [2048], P('kv'), may hold values from 0.1 to 1.9
- w_query: bfloat16 [2048, 2048], P('kv', 'tp'), may hold values from -0.25 to 0.25
- w_key: bfloat16 [2048, 2048], P('kv', 'tp'), may hold values from -0.125 to 0.125
- w_value: bfloat16 [2048, 2048], P('kv', 'tp'), may hold values from -0.125 to 0.125
- w_output: bfloat16 [2048, 2048], P('tp', 'kv'), may hold values from -0.125 to 0.125
- key_cache: bfloat16 [16, 16384, 16, 128], P('dp', 'kv', 'tp'), may hold values from -170 to 170
- value_cache: bfloat16 [16, 16384, 16, 128], P('dp', 'kv', 'tp'), may hold values from -6 to 6
- lengths: int32 [16], P('dp'), may hold values from 8192 to 16383, as said below
- lam: float32 [16], P('tp'), may hold values from 0.3 to 0.8
- head_gain: float32 [128], replicated, may hold values from 0.1 to 1.9
Outputs:
- attended: bfloat16 [16, 2048], P('dp', 'kv')
- new_key: bfloat16 [16, 2048], P('dp', 'tp')
- new_value: bfloat16 [16, 2048], P('dp', 'tp')
Inputs may be any that keep to these rules, and one draw needn't show every extreme that they name: `lengths`: exactly one sequence, chosen by the draw, has 16383 past tokens.
All inputs are finite; a program needn't handle non-finite values.
Results may differ from a plain program's by a relative error of at most 0.012.
Values may be sent and summed in bfloat16 or wider, within the bound.
No kernel may reach another device: no remote copies, remote signals or barrier semaphores. Data moves between devices by JAX's collectives and lax.ppermute only.
A program may use at most 64 MiB of HBM per device.

v0:
```python
import jax
import jax.numpy as jnp
from jax import lax
from jax.sharding import Mesh
from jax.sharding import PartitionSpec as P

D = 2048
HEAD_WIDTH = 64
VDIM = 128
KV = ("kv_0", "kv_1")


epsilon = 1e-06


def from_everyone(array, axis):
    copies = jnp.broadcast_to(array, (lax.axis_size(axis), *array.shape))
    return lax.all_to_all(copies, axis, split_axis=0, concat_axis=0, tiled=True)


def taken_together(array, axis):
    everything = from_everyone(array, axis)
    return jnp.sum(everything, axis=0)


def packed_total(arrays, axis):
    ends = [0]
    for a in arrays:
        ends.append(ends[-1] + a.size)
    so_far = taken_together(jnp.concatenate([a.ravel() for a in arrays]), axis)
    return tuple((so_far[b:e].reshape(a.shape) for a, b, e in zip(arrays, ends, ends[1:])))


def collected_together(array, axis):
    leaves = jax.tree.leaves(array)
    turns = sorted(range(len(leaves)), key=lambda k: -leaves[k].size)
    width = (1, *leaves[turns[0]].shape)[-1]
    lines = [
        jnp.pad(leaves[k].reshape(-1), (0, -leaves[k].size % width)).reshape(-1, width)
        for k in turns
    ]
    both, at, found = (lax.all_gather(jnp.concatenate(lines), axis), 0, {})
    for k, line in zip(turns, lines):
        share = both[:, at : at + len(line)].reshape(len(both), -1)
        found[k] = share[:, : leaves[k].size].reshape(-1, *leaves[k].shape)
        at += len(line)
    numbers = iter(range(len(leaves)))
    return jax.tree.map(lambda _: found[next(numbers)], array)


def combined_by_axis(array, axes, combine):
    for axis in axes:
        pieces = collected_together(array, axis)
        array = jax.tree.map(lambda part: part[0], pieces)
        for k in range(1, lax.axis_size(axis)):
            array = combine(array, jax.tree.map(lambda part: part[k], pieces))
    return array


def gathered_total(array, axis):
    return lax.all_gather(array, axis).astype(jnp.float32).sum(0)


def combine_parts(earlier, later):
    top = jnp.maximum(earlier[0], later[0])
    first = jnp.exp(earlier[0] - top)
    second = jnp.exp(later[0] - top)
    total = earlier[1] * first + later[1] * second
    summed = earlier[2] * first[..., None] + later[2] * second[..., None]
    return (top, total, summed)


def per_device(
    tokens,
    norm_gain,
    w_query,
    w_key,
    w_value,
    w_output,
    key_cache,
    value_cache,
    lengths,
    lam,
    head_gain,
):
    seqs = tokens.shape[0]
    heads_here = lam.shape[0]
    span = key_cache.shape[1]
    xfull = tokens.astype(jnp.float32)
    squares = jnp.sum(xfull * xfull, axis=-1)
    scaled = (xfull * norm_gain).astype(jnp.bfloat16)
    part_query = jnp.dot(scaled, w_query, preferred_element_type=jnp.float32)
    part_key = jnp.dot(scaled, w_key, preferred_element_type=jnp.float32)
    part_value = jnp.dot(scaled, w_value, preferred_element_type=jnp.float32)
    part_query, part_key, part_value, squares = packed_total(
        (part_query, part_key, part_value, squares), KV
    )
    inv = lax.rsqrt(squares / D + epsilon)[:, None]
    query = (part_query * inv).astype(jnp.bfloat16)
    new_key = (part_key * inv).astype(jnp.bfloat16)
    new_value = (part_value * inv).astype(jnp.bfloat16)
    positions = lax.axis_index(KV) * span + jnp.arange(span, dtype=jnp.int32)
    hit = (positions[None, :] == lengths[:, None])[:, :, None, None]
    key_rows = jnp.where(hit, new_key.reshape(seqs, 1, heads_here, 2 * HEAD_WIDTH), key_cache)
    values = jnp.where(hit, new_value.reshape(seqs, 1, heads_here, VDIM), value_cache)
    logit_score = jnp.einsum(
        "bhmd,bphmd->bhmp",
        query.reshape(seqs, heads_here, 2, HEAD_WIDTH),
        key_rows.reshape(seqs, span, heads_here, 2, HEAD_WIDTH),
        preferred_element_type=jnp.float32,
    ) * HEAD_WIDTH ** (-0.5)
    live = (positions[None, :] <= lengths[:, None])[:, None, None, :]
    masked = jnp.where(live, logit_score, jnp.float32(-1e30))
    block_peak = jnp.max(masked, axis=-1)
    weights = jnp.where(live, jnp.exp(masked - block_peak[..., None]), jnp.float32(0.0))
    block_sum = jnp.sum(weights, axis=-1)
    acc = jnp.einsum(
        "bhmp,bphv->bhmv", weights.astype(jnp.bfloat16), values, preferred_element_type=jnp.float32
    )
    scale_lam = lam[None, :, None]
    top, total, summed = combined_by_axis((block_peak, block_sum, acc), KV, combine_parts)
    mixed = (
        summed[:, :, 0] / total[:, :, 0, None] - scale_lam * summed[:, :, 1] / total[:, :, 1, None]
    )
    normed = (
        mixed * lax.rsqrt(jnp.mean(mixed * mixed, axis=-1, keepdims=True) + epsilon) * head_gain
    )
    heads = normed.astype(jnp.bfloat16).reshape(seqs, heads_here * VDIM)
    partial_value = jnp.dot(heads, w_output, preferred_element_type=jnp.float32).astype(
        jnp.bfloat16
    )
    attended = gathered_total(partial_value, "tp").astype(jnp.float32).astype(jnp.bfloat16)
    return (attended, new_key, new_value)


def solution(mesh):
    split = Mesh(
        mesh.devices.reshape(mesh.shape["dp"], 8, 4, mesh.shape["tp"]), ("dp", "kv_0", "kv_1", "tp")
    )
    return jax.shard_map(
        per_device,
        mesh=split,
        in_specs=(
            P("dp", KV),
            P(KV),
            P(KV, "tp"),
            P(KV, "tp"),
            P(KV, "tp"),
            P("tp", KV),
            P("dp", KV, "tp", None),
            P("dp", KV, "tp", None),
            P("dp"),
            P("tp"),
            P(),
        ),
        out_specs=(P("dp", KV), P("dp", "tp"), P("dp", "tp")),
        check_vma=False,
    )
```

profile of v0, /device:TPU:1, one launch (start us, length us, event | category | flops | bytes accessed | tf_op | source)
XLA Modules:
  0.0 110.4 jit_solution(10117884581644328169)
XLA Ops:
  0.6 0.0 copy-start
  0.6 0.8 fusion.43
  1.5 0.1 copy-done
  1.6 0.8 convolution_bitcast_fusion.2
  2.4 1.1 convolution_bitcast_fusion.1
  3.4 1.1 convolution_bitcast_fusion
  4.5 2.1 %broadcast_in_dim.45 = f32[32,1,12292]{2,1,0:T(1,128)} broadcast(f32[12292]{0:T(1024)S(1)} %pad_maximum_fusion), dimensions={2} | broadcast | bytes 1622544 | tf_op jit(solution)/shard_map/broadcast_in_dim | solution.py:17
  6.6 12.0 %all-to-all-start = ((f32[32,1,12292]{2,1,0:T(1,128)}), f32[32,1,12292]{2,1,0:T(1,128)S(1)}, u32[]{:S(2)}, u32[]{:S(2)}) async-start(f32[32,1,12292]{2,1,0:T(1,128)} %broadcast_in_dim.45), calls=%async_computation | async-start | bytes 3178496 | tf_op jit(solution)/shard_map/all_to_all | solution.py:18
  18.6 7.5 %copy.29 = bf16[4,512,8,128]{1,3,2,0:T(8,128)(2,1)} copy(bf16[4,512,8,128]{3,2,1,0:T(8,128)(2,1)} %param.17) | data formatting | bytes 8388608 | tf_op args[6]
  26.2 0.0 copy-start.3
  26.2 0.0 copy-start.1
  26.2 0.0 copy-start.2
  26.2 7.6 %copy.30 = bf16[4,512,8,128]{1,3,2,0:T(8,128)(2,1)} copy(bf16[4,512,8,128]{3,2,1,0:T(8,128)(2,1)} %param.18) | data formatting | bytes 8388608 | tf_op args[7]
  33.8 0.0 copy-done.3
  33.8 0.1 broadcast_compare_fusion.1
  33.8 0.0 copy-done.1
  33.8 0.0 copy-done.2
  33.8 0.1 broadcast_bitcast_fusion.3
  33.9 22.9 %all-to-all-done = f32[32,1,12292]{2,1,0:T(1,128)S(1)} async-done(((f32[32,1,12292]{2,1,0:T(1,128)}), f32[32,1,12292]{2,1,0:T(1,128)S(1)}, u32[]{:S(2)}, u32[]{:S(2)}) %all-to-all-start) | async-done | bytes 1573408 | tf_op jit(solution)/shard_map/all_to_all | solution.py:18
  56.8 0.9 reduce_sum.49
  57.7 0.1 fusion.36
  57.8 0.1 reshape.679
  57.9 0.1 fusion.38
  58.0 2.6 %broadcast_select_fusion = bf16[4,512,8,128]{1,3,2,0:T(8,128)(2,1)S(1)} fusion(bf16[4,512,8,128]{1,3,2,0:T(8,128)(2,1)} %copy.29, pred[4,512]{1,0:T(4,128)(4,1)S(1)} %get-tuple-element.56, bf16[4,8,128]{2,1,0:T(8,128)(2,1)S(1)} %get-tuple-element.48), kind=kLoop, calls=%fused_computation.3 | loop fusion | flops 2097152 | bytes 8398848 | tf_op jit(solution)/shard_map/jit(_where)/select_n | solution.py:104
  60.6 0.6 fusion.29
  61.2 0.2 fusion.7
  61.4 0.1 reshape.684
  61.5 0.3 fusion.70
  61.8 0.1 reshape.686
  61.9 0.0 copy-start.4
  61.9 3.5 %fusion = f32[4,8,2,128]{3,2,1,0:T(2,128)S(1)} fusion(bf16[4,512,8,128]{1,3,2,0:T(8,128)(2,1)} %copy.30, pred[4,512]{1,0:T(4,128)(4,1)S(1)} %get-tuple-element.56, bf16[4,8,128]{2,1,0:T(8,128)(2,1)S(1)} %get-tuple-element.47, pred[4,512]{1,0:T(4,128)(4,1)S(1)} %get-tuple-element.55, f32[4,8,2]{2,1,0:T(8,128)S(1)} %fusion.7, f32[4,8,2,1,512]{4,3,2,1,0:T(1,128)S(1)} %fusion.29), kind=kOutput, calls=%fused_computation | convolution fusion | flops 10649600 | bytes 4370688 | tf_op jit(solution)/shard_map/bhmp,bphv->bhmv/dot_general | solution.py:117
  65.4 18.8 %all-gather.3 = f32[8,66,128]{2,1,0:T(8,128)S(1)} all-gather(f32[1,66,128]{2,1,0:T(8,128)S(1)} %maximum_bitcast_fusion), channel_id=2, replica_groups=mesh['dp'=4,'kv_0'=8,'kv_1'=4,'tp'=2] {'kv_0'}, dimensions={0}, use_global_device_ids=true | all-gather | bytes 304128 | tf_op jit(solution)/shard_map/all_gather | solution.py:42
  84.3 0.2 fusion.9
  84.5 10.8 %all-gather.4 = f32[4,66,128]{2,1,0:T(8,128)S(1)} all-gather(f32[1,66,128]{2,1,0:T(8,128)S(1)} %maximum_bitcast_fusion.1), channel_id=3, replica_groups=mesh['dp'=4,'kv_0'=8,'kv_1'=4,'tp'=2] {'kv_1'}, dimensions={0}, use_global_device_ids=true | all-gather | bytes 168960 | tf_op jit(solution)/shard_map/all_gather | solution.py:42
  95.3 0.1 squeeze.151
  95.4 0.1 squeeze.154
  95.6 0.1 squeeze.153
  95.7 0.1 squeeze.152
  95.8 0.1 squeeze.143
  95.9 0.1 squeeze.144
  96.0 0.1 squeeze.148
  96.1 0.1 squeeze.146
  96.2 0.1 slice_reduce_fusion.1
  96.4 0.3 multiply_add_fusion
  96.7 0.1 slice_reduce_fusion.10
  96.7 0.2 broadcast_bitcast_fusion.2
  96.9 0.1 broadcast_bitcast_fusion
  97.0 0.0 copy-done.4
  97.0 0.2 fusion.4
  97.1 12.0 %all-gather.5 = bf16[2,4,64]{2,1,0:T(4,128)(2,1)S(1)} all-gather(bf16[1,4,64]{2,1,0:T(4,128)(2,1)S(1)} %fusion.4), channel_id=4, replica_groups=mesh['dp'=4,'kv_0'=8,'kv_1'=4,'tp'=2] {'tp'}, dimensions={0}, use_global_device_ids=true | all-gather | bytes 1536 | tf_op jit(solution)/shard_map/all_gather | solution.py:61
  109.2 0.7 multiply_convert_fusion.1
  109.8 0.6 reduce_sum.52
  (23 shorter events, 0.2 us)
Async XLA Ops:
  0.6 0.9 copy-start
  6.6 50.2 %all-to-all-start = ((f32[32,1,12292]{2,1,0:T(1,128)}), f32[32,1,12292]{2,1,0:T(1,128)S(1)}, u32[]{:S(2)}, u32[]{:S(2)}) async-start(f32[32,1,12292]{2,1,0:T(1,128)} %broadcast_in_dim.45), calls=%async_computation | async-start | bytes 3178496 | tf_op jit(solution)/shard_map/all_to_all | solution.py:18
  26.2 7.6 %copy-start.3 = (s32[4]{0:T(128)S(1)}, s32[4]{0:T(128)}, u32[]{:S(2)}) copy-start(s32[4]{0:T(128)} %param.19) | copy-start | bytes 52
  26.2 7.7 %copy-start.1 = (f32[8]{0:T(128)S(1)}, f32[8]{0:T(128)}, u32[]{:S(2)}) copy-start(f32[8]{0:T(128)} %param.20) | copy-start | bytes 100
  26.2 7.7 %copy-start.2 = (f32[128]{0:T(128)S(1)}, f32[128]{0:T(128)}, u32[]{:S(2)}) copy-start(f32[128]{0:T(128)} %param.21) | copy-start | bytes 1540
  61.9 35.1 %copy-start.4 = (bf16[1024,64]{0,1:T(8,128)(2,1)S(1)}, bf16[1024,64]{0,1:T(8,128)(2,1)}, u32[]{:S(2)}) copy-start(bf16[1024,64]{0,1:T(8,128)(2,1)} %param.16) | copy-start | bytes 393220
where the time goes:
time: 111 us; the launch traced here: 110 us
  blocking collectives  41.5 us (37%)
  waiting for transfers between devices  22.9 us (21%)
  local copies, waits for them, and re-layouts  18.8 us (17%)
  starting transfers between devices  12 us (11%)
  matrix products  7.23 us (7%)
  other arithmetic  7.02 us (6%)
    all_gather x2, blocking collectives, collected_together(): both, at, found = (lax.all_gather(jnp.concatenate(lines), axis), 0, {})  29.5 us
    all_to_all x1, waiting for transfers between devices, from_everyone(): return lax.all_to_all(copies, axis, split_axis=0, concat_axis=0, tiled=True)  22.9 us
    unnamed x16, local copies, waits for them, and re-layouts  15.3 us
    all_to_all x1, starting transfers between devices, from_everyone(): return lax.all_to_all(copies, axis, split_axis=0, concat_axis=0, tiled=True)  12 us
    all_gather x1, blocking collectives, gathered_total(): return lax.all_gather(array, axis).astype(jnp.float32).sum(0)  12 us
    dot_general x1, matrix products, per_device(): jnp.einsum('bhmp,bphv->bhmv', weights.astype(jnp.bfloat16), values, prefe...  3.48 us
    select_n x1, other arithmetic, per_device(): jnp.where(hit, new_key.reshape(seqs, 1, heads_here, 2 * HEAD_WIDTH), key_...  2.59 us
  transfers between devices with their start and end apart: 1, of which 1 were waited for; matrix products, arithmetic and copies ran while one was open for 14% of the time, Pallas kernels for 0%

commit v1 on v0

v1 whole, which is shorter than its diff:
```python
import functools

import jax
import jax.numpy as jnp
from jax import lax
from jax.experimental import pallas as pl
from jax.experimental.pallas import tpu as pltpu
from jax.sharding import PartitionSpec as P

D = 2048
HEAD_WIDTH = 64
EPS = 1e-6
NEG = -1e30

ROW_K, ROW_V, ROW_SQ, ROWS_A = 32, 33, 36, 40
ROW_M, ROW_L, ROW_S, ROW_NK, ROW_NV, ROWS_C = 64, 66, 68, 70, 71, 72


def project(tok_ref, gain_ref, wq_ref, wk_ref, wv_ref, out_ref):
    peers = out_ref.shape[0]
    x = tok_ref[...].astype(jnp.float32)
    seqs = x.shape[0]
    squares = jnp.sum(x * x, axis=-1, keepdims=True)
    scaled = (x * gain_ref[...]).astype(jnp.bfloat16)
    heads = wq_ref.shape[1] // 128

    def rows(w_ref):
        y = jnp.dot(scaled, w_ref[...], preferred_element_type=jnp.float32)
        return jnp.concatenate([y[:, h * 128 : (h + 1) * 128] for h in range(heads)], axis=0)

    q, k, v = rows(wq_ref), rows(wk_ref), rows(wv_ref)
    sq = jnp.broadcast_to(squares, (seqs, 128))
    for j in range(peers):
        out_ref[j, 0:32, :] = q
        out_ref[j, ROW_K : ROW_K + 1, :] = k[j : j + 1, :]
        out_ref[j, ROW_V : ROW_V + 1, :] = v[j : j + 1, :]
        out_ref[j, ROW_SQ : ROW_SQ + seqs, :] = sq


def two_pieces(a):
    hi = a.astype(jnp.bfloat16).astype(jnp.float32)
    return hi, (a - hi).astype(jnp.bfloat16).astype(jnp.float32)


def attend(got_ref, key_ref, val_ref, len_ref, out_ref, q_scr, col_scr):
    peers = got_ref.shape[0]
    seqs = key_ref.shape[0]
    width = key_ref.shape[1]
    span = width // 8
    me = lax.axis_index("kv")
    total = got_ref[0]
    for j in range(1, peers):
        total = total + got_ref[j]
    inv = lax.rsqrt(total[ROW_SQ : ROW_SQ + seqs] / D + EPS)
    inv8 = jnp.concatenate([inv, inv], axis=0)
    inv32 = jnp.concatenate([inv8] * 4, axis=0)
    q = (total[0:32] * inv32).astype(jnp.bfloat16).astype(jnp.float32)
    q_scr[...] = q
    seq_id = lax.broadcasted_iota(jnp.int32, (seqs, 128), 0)
    mine = jnp.sum(jnp.where(seq_id == lax.rem(me, seqs), inv, 0.0), axis=0, keepdims=True)
    nk = (total[ROW_K : ROW_K + 1] * mine).astype(jnp.bfloat16)
    nv = (total[ROW_V : ROW_V + 1] * mine).astype(jnp.bfloat16)
    lane = lax.broadcasted_iota(jnp.int32, (8, 128), 1)
    sub = lax.broadcasted_iota(jnp.int32, (8, 128), 0)
    lane1 = lax.broadcasted_iota(jnp.int32, (1, 128), 1)
    qk = q_scr[pl.ds(me, 1), :] * nk.astype(jnp.float32) * HEAD_WIDTH**-0.5
    s1 = jnp.sum(jnp.where(lane1 < HEAD_WIDTH, qk, 0.0), axis=1, keepdims=True)
    s2 = jnp.sum(jnp.where(lane1 >= HEAD_WIDTH, qk, 0.0), axis=1, keepdims=True)
    spot = lax.rem(me, seqs) * 16 + me // seqs
    snew = jnp.where(lane1 == spot, s1, jnp.where(lane1 == spot + 8, s2, NEG))
    own_head = lax.rem(lane, 8) == sub
    col = lax.broadcasted_iota(jnp.int32, (8, width), 1)
    own_head_wide = lax.rem(col, 8) == lax.broadcasted_iota(jnp.int32, (8, width), 0)
    accs = []
    for b in range(seqs):
        qb = q_scr[pl.ds(b, 8, stride=seqs), :] * HEAD_WIDTH**-0.5
        q1 = jnp.where(lane < HEAD_WIDTH, qb, 0.0)
        q2 = jnp.where(lane >= HEAD_WIDTH, qb, 0.0)
        q16 = jnp.concatenate([q1, q2], axis=0).astype(jnp.bfloat16)
        s = lax.dot_general(
            q16, key_ref[b], (((1,), (1,)), ((), ())), preferred_element_type=jnp.float32
        )
        limit = (len_ref[b] - me * span) * 8
        live = jnp.logical_and(own_head_wide, col < limit)
        weights = []
        for m in range(2):
            part = jnp.where(live, s[m * 8 : (m + 1) * 8], NEG)
            hi, lo = two_pieces(jnp.max(part, axis=1, keepdims=True))
            w = jnp.where(live, jnp.exp(part - (hi + lo)), 0.0)
            lhi, llo = two_pieces(jnp.sum(w, axis=1, keepdims=True))
            weights.append(w)
            r = b * 16 + m * 8
            col_scr[r : r + 8, :] = jnp.where(
                lane == 0, hi, jnp.where(lane == 1, lo, jnp.where(lane == 2, lhi, llo))
            )
        w16 = jnp.concatenate(weights, axis=0).astype(jnp.bfloat16)
        accs.append(jnp.dot(w16, val_ref[b], preferred_element_type=jnp.float32))
    turned = jnp.concatenate([col_scr[...], jnp.zeros_like(col_scr)], axis=0).T
    shi, slo = two_pieces(snew)
    tail = jnp.concatenate(
        [turned[0:4], shi, slo, nk.astype(jnp.float32), nv.astype(jnp.float32)], axis=0
    )
    packed = jnp.concatenate(accs + [tail], axis=0).astype(jnp.bfloat16)
    for j in range(peers):
        out_ref[j] = packed


def merge(got_ref, lam_ref, gain_ref, wo_ref, part_ref, nk_ref, nv_ref, head_scr, v_scr):
    peers = got_ref.shape[0]
    seqs = nk_ref.shape[0]

    def row(r):
        return jnp.concatenate(
            [got_ref[j, ROW_M:ROWS_C, :].astype(jnp.float32)[r - ROW_M : r - ROW_M + 1] for j in range(peers)],
            axis=0,
        )

    top = row(ROW_M) + row(ROW_M + 1)
    part = row(ROW_L) + row(ROW_L + 1)
    snew = row(ROW_S) + row(ROW_S + 1)
    peak = jnp.maximum(
        jnp.max(top, axis=0, keepdims=True), jnp.max(snew, axis=0, keepdims=True)
    )
    factor = jnp.exp(top - peak)
    fresh = jnp.sum(jnp.exp(snew - peak), axis=0, keepdims=True)
    total = jnp.sum(part * factor, axis=0, keepdims=True) + fresh
    scale = jnp.concatenate(
        [factor / total, jnp.broadcast_to(fresh / total, (8, 128)), jnp.zeros((88, 128), jnp.float32)],
        axis=0,
    ).T
    nk = row(ROW_NK)
    nv = row(ROW_NV)
    v_scr[...] = nv
    for h in range(8):
        nk_ref[:, h * 128 : (h + 1) * 128] = nk[h * seqs : (h + 1) * seqs].astype(jnp.bfloat16)
        nv_ref[:, h * 128 : (h + 1) * 128] = nv[h * seqs : (h + 1) * seqs].astype(jnp.bfloat16)
    for b in range(seqs):
        maps = []
        fresh_v = v_scr[pl.ds(b, 8, stride=seqs), :]
        for m in range(2):
            r = b * 16 + m * 8
            acc = scale[r : r + 8, peers : peers + 1] * fresh_v
            for j in range(peers):
                acc = acc + scale[r : r + 8, j : j + 1] * got_ref[j, r : r + 8, :].astype(jnp.float32)
            maps.append(acc)
        mixed = maps[0] - lam_ref[...] * maps[1]
        mean = jnp.mean(mixed * mixed, axis=1, keepdims=True)
        head_scr[b * 8 : b * 8 + 8, :] = mixed * lax.rsqrt(mean + EPS) * gain_ref[...]
    heads = jnp.concatenate(
        [head_scr[pl.ds(h, seqs, stride=8), :] for h in range(8)], axis=1
    ).astype(jnp.bfloat16)
    part_ref[...] = jnp.dot(heads, wo_ref[...], preferred_element_type=jnp.float32).astype(
        jnp.bfloat16
    )


VM = pl.BlockSpec(memory_space=pltpu.VMEM)
SM = pl.BlockSpec(memory_space=pltpu.SMEM)


def exchange(array):
    return lax.all_to_all(array, "kv", split_axis=0, concat_axis=0, tiled=True)


def per_device(
    tokens, norm_gain, w_query, w_key, w_value, w_output, key_cache, value_cache, lengths, lam, head_gain
):
    peers = lax.axis_size("kv")
    seqs, span, heads, width = key_cache.shape
    sent = pl.pallas_call(
        project,
        out_shape=jax.ShapeDtypeStruct((peers, ROWS_A, 128), jnp.float32),
        in_specs=[VM] * 5,
        out_specs=VM,
        name="project",
    )(tokens, norm_gain.reshape(1, -1), w_query, w_key, w_value)
    got = exchange(sent)
    sent = pl.pallas_call(
        attend,
        out_shape=jax.ShapeDtypeStruct((peers, ROWS_C, 128), jnp.bfloat16),
        in_specs=[VM, VM, VM, SM],
        out_specs=VM,
        scratch_shapes=[
            pltpu.VMEM((32, 128), jnp.float32),
            pltpu.VMEM((64, 128), jnp.float32),
        ],
        name="attend",
    )(
        got,
        key_cache.reshape(seqs, span * heads, width),
        value_cache.reshape(seqs, span * heads, width),
        lengths,
    )
    got = exchange(sent)
    part, new_key, new_value = pl.pallas_call(
        merge,
        out_shape=(
            jax.ShapeDtypeStruct((seqs, w_output.shape[1]), jnp.bfloat16),
            jax.ShapeDtypeStruct((seqs, heads * width), jnp.bfloat16),
            jax.ShapeDtypeStruct((seqs, heads * width), jnp.bfloat16),
        ),
        in_specs=[VM] * 4,
        out_specs=(VM, VM, VM),
        scratch_shapes=[
            pltpu.VMEM((32, 128), jnp.float32),
            pltpu.VMEM((32, 128), jnp.float32),
        ],
        name="merge",
    )(
        got,
        jnp.broadcast_to(lam[:, None], (heads, 128)),
        head_gain.reshape(1, -1),
        w_output,
    )
    both = lax.all_gather(part, "tp")
    attended = jnp.sum(both.astype(jnp.float32), axis=0).astype(jnp.bfloat16)
    return (attended, new_key, new_value)


def solution(mesh):
    return jax.shard_map(
        per_device,
        mesh=mesh,
        in_specs=(
            P("dp", "kv"),
            P("kv"),
            P("kv", "tp"),
            P("kv", "tp"),
            P("kv", "tp"),
            P("tp", "kv"),
            P("dp", "kv", "tp", None),
            P("dp", "kv", "tp", None),
            P("dp"),
            P("tp"),
            P(),
        ),
        out_specs=(P("dp", "kv"), P("dp", "tp"), P("dp", "tp")),
        check_vma=False,
    )
```

time: 111 us -> 72.5 us (0.65)
  local copies, waits for them, and re-layouts: 18.8 us -> 1.67 us
  Pallas kernels: 0 us -> 12 us
  matrix products: 7.23 us -> 0 us
  waiting for transfers between devices: 22.9 us -> 15.8 us
  starting transfers between devices: 12 us -> 5.54 us
  other arithmetic: 7.02 us -> 0.57 us
  blocking collectives: 41.5 us -> 36 us
    all_gather x3 -> x1, blocking collectives: 41.5 us -> 5.18 us  [per_device(): both = lax.all_gather(part, 'tp')]
    all_to_all x0 -> x1, blocking collectives: none -> 30.8 us  [exchange(): return lax.all_to_all(array, 'kv', split_axis=0, concat_axis=0, tiled=True)]
    unnamed x16 -> x7, local copies, waits for them, and re-layouts: 15.3 us -> 0.91 us
    pallas_call x0 -> x3, Pallas kernels: none -> 12 us  [the longest x1 7.19 us: per_device(): pl.pallas_call(attend, out_shape=jax.ShapeDtypeStruct((peers, ROWS_C, 128...]
    dot_general x6 -> x0, matrix products: 7.23 us -> none  [the longest x1 3.48 us: per_device(): jnp.einsum('bhmp,bphv->bhmv', weights.astype(jnp.bfloat16), values, prefe...]
    all_to_all x1, waiting for transfers between devices: 22.9 us -> 15.8 us  [exchange(): return lax.all_to_all(array, 'kv', split_axis=0, concat_axis=0, tiled=True)]
    all_to_all x1, starting transfers between devices: 12 us -> 5.54 us  [exchange(): return lax.all_to_all(array, 'kv', split_axis=0, concat_axis=0, tiled=True)]
    select_n x1 -> x0, other arithmetic: 2.59 us -> none  [per_device(): jnp.where(hit, new_key.reshape(seqs, 1, heads_here, 2 * HEAD_WIDTH), key_...]
  transfers between devices with their start and end apart: 1 -> 1, of which waited for: 1 -> 1; matrix products, arithmetic and copies ran while one was open for 14% -> 1% of each run, Pallas kernels for 0% -> 0%
where the time goes in v1:
time: 72.5 us; the launch traced here: 72.1 us
  blocking collectives  36 us (50%)
  waiting for transfers between devices  15.8 us (22%)
  Pallas kernels  12 us (17%)
  starting transfers between devices  5.54 us (8%)
  local copies, waits for them, and re-layouts  1.67 us (2%)
    all_to_all x1, blocking collectives, exchange(): return lax.all_to_all(array, 'kv', split_axis=0, concat_axis=0, tiled=True)  30.8 us
    all_to_all x1, waiting for transfers between devices, exchange(): return lax.all_to_all(array, 'kv', split_axis=0, concat_axis=0, tiled=True)  15.8 us
    pallas_call x1, Pallas kernels, per_device(): pl.pallas_call(attend, out_shape=jax.ShapeDtypeStruct((peers, ROWS_C, 128...  7.19 us
    all_to_all x1, starting transfers between devices, exchange(): return lax.all_to_all(array, 'kv', split_axis=0, concat_axis=0, tiled=True)  5.54 us
    all_gather x1, blocking collectives, per_device(): both = lax.all_gather(part, 'tp')  5.18 us
    pallas_call x1, Pallas kernels, per_device(): pl.pallas_call(merge, out_shape=(jax.ShapeDtypeStruct((seqs, w_output.sha...  2.7 us
    pallas_call x1, Pallas kernels, per_device(): pl.pallas_call(project, out_shape=jax.ShapeDtypeStruct((peers, ROWS_A, 12...  2.08 us
  transfers between devices with their start and end apart: 1, of which 1 were waited for; matrix products, arithmetic and copies ran while one was open for 1% of the time, Pallas kernels for 0%

profile of v1, /device:TPU:1, one launch (start us, length us, event | category | flops | bytes accessed | tf_op | source)
XLA Modules:
  0.0 72.1 jit_solution(16883632577554719297)
XLA Ops:
  0.6 2.1 %project.1 = f32[32,40,128]{2,1,0:T(8,128)} custom-call(bf16[4,64]{1,0:T(4,128)(2,1)} %tok_ref.1, f32[1,64]{1,0:T(1,128)} %bitcast.8, bf16[64,1024]{1,0:T(8,128)(2,1)} %wq_ref.1, bf16[64,1024]{1,0:T(8,128)(2,1)} %wk_ref.1, bf16[64,1024]{1,0:T(8,128)(2,1)} %wv_ref.1), custom_call_target="tpu_custom_call" | custom-call | tf_op jit(solution)/shard_map/project/pallas_call | solution.py:170
  2.7 30.8 %all_to_all.10.got_ref = f32[32,40,128]{2,1,0:T(8,128)} all-to-all(f32[32,40,128]{2,1,0:T(8,128)} %project.1), channel_id=1, replica_groups=mesh['dp'=4,'kv'=32,'tp'=2] {'kv'}, dimensions={0} | all-to-all | bytes 1310720 | tf_op jit(solution)/shard_map/all_to_all | solution.py:162
  33.5 0.0 copy-start.1
  33.5 0.0 copy-start.2
  33.5 7.2 %attend.1 = bf16[32,72,128]{2,1,0:T(8,128)(2,1)} custom-call(f32[32,40,128]{2,1,0:T(8,128)} %all_to_all.10.got_ref, bf16[4,4096,128]{2,1,0:T(8,128)(2,1)} %bitcast.5, bf16[4,4096,128]{2,1,0:T(8,128)(2,1)} %bitcast.6, s32[4]{0:T(128)} %len_ref.1), custom_call_target="tpu_custom_call" | custom-call | tf_op jit(solution)/shard_map/attend/pallas_call | solution.py:178
  40.7 5.5 %all-to-all-start.1 = ((bf16[32,72,128]{2,1,0:T(8,128)(2,1)}), bf16[32,72,128]{2,1,0:T(8,128)(2,1)S(1)}, u32[]{:S(2)}, u32[]{:S(2)}) async-start(bf16[32,72,128]{2,1,0:T(8,128)(2,1)} %attend.1), calls=%async_computation.1 | async-start | bytes 1179648 | tf_op jit(solution)/shard_map/all_to_all | solution.py:162
  46.3 0.0 copy-done.1
  46.3 0.8 %copy.15.wo_ref = bf16[1024,64]{1,0:T(8,128)(2,1)} copy(bf16[1024,64]{0,1:T(8,128)(2,1)S(1)} %copy-done.1) | data formatting | bytes 262144 | tf_op args[5]
  47.1 15.8 %all-to-all-done.1.got_ref = bf16[32,72,128]{2,1,0:T(8,128)(2,1)S(1)} async-done(((bf16[32,72,128]{2,1,0:T(8,128)(2,1)}), bf16[32,72,128]{2,1,0:T(8,128)(2,1)S(1)}, u32[]{:S(2)}, u32[]{:S(2)}) %all-to-all-start.1) | async-done | bytes 589856 | tf_op jit(solution)/shard_map/all_to_all | solution.py:162
  62.9 0.0 copy-done.2
  62.9 0.0 copy-start
  62.9 0.8 %broadcast_in_dim.2.lam_ref = f32[8,128]{1,0:T(8,128)} broadcast(f32[8]{0:T(128)S(1)} %copy-done.2), dimensions={0} | broadcast | bytes 4128 | tf_op jit(solution)/shard_map/broadcast_in_dim | solution.py:211
  63.6 0.1 copy-done
  63.7 2.7 %merge.1 = (bf16[4,64]{1,0:T(4,128)(2,1)}, bf16[4,1024]{1,0:T(4,128)(2,1)}, bf16[4,1024]{1,0:T(4,128)(2,1)}) custom-call(bf16[32,72,128]{2,1,0:T(8,128)(2,1)} %copy-done, f32[8,128]{1,0:T(8,128)} %broadcast_in_dim.2.lam_ref, f32[1,128]{1,0:T(1,128)} %bitcast.9, bf16[1024,64]{1,0:T(8,128)(2,1)} %copy.15.wo_ref), custom_call_target="tpu_custom_call" | custom-call | tf_op jit(solution)/shard_map/merge/pallas_call | solution.py:195
  66.4 5.2 %all-gather.1 = bf16[2,4,64]{2,1,0:T(4,128)(2,1)S(1)} all-gather(bf16[1,4,64]{2,1,0:T(4,128)(2,1)} %bitcast.7), channel_id=2, replica_groups=mesh['dp'=4,'kv'=32,'tp'=2] {'tp'}, dimensions={0}, use_global_device_ids=true | all-gather | bytes 1536 | tf_op jit(solution)/shard_map/all_gather | solution.py:215
  71.6 0.6 reduce_sum.12
Async XLA Ops:
  33.5 12.7 %copy-start.1 = (bf16[1024,64]{0,1:T(8,128)(2,1)S(1)}, bf16[1024,64]{0,1:T(8,128)(2,1)}, u32[]{:S(2)}) copy-start(bf16[1024,64]{0,1:T(8,128)(2,1)} %param.16) | copy-start | bytes 393220
  33.5 29.3 %copy-start.2 = (f32[8]{0:T(128)S(1)}, f32[8]{0:T(128)}, u32[]{:S(2)}) copy-start(f32[8]{0:T(128)} %param.20) | copy-start | bytes 100
  40.7 22.1 %all-to-all-start.1 = ((bf16[32,72,128]{2,1,0:T(8,128)(2,1)}), bf16[32,72,128]{2,1,0:T(8,128)(2,1)S(1)}, u32[]{:S(2)}, u32[]{:S(2)}) async-start(bf16[32,72,128]{2,1,0:T(8,128)(2,1)} %attend.1), calls=%async_computation.1 | async-start | bytes 1179648 | tf_op jit(solution)/shard_map/all_to_all | solution.py:162
  62.9 0.8 %copy-start = (bf16[32,72,128]{2,1,0:T(8,128)(2,1)}, bf16[32,72,128]{2,1,0:T(8,128)(2,1)S(1)}, u32[]{:S(2)}) copy-start(bf16[32,72,128]{2,1,0:T(8,128)(2,1)S(1)} %all-to-all-done.1.got_ref) | copy-start | bytes 1769476

commit v2 on v1

--- a/solution.py
+++ b/solution.py
@@ -16,7 +16,17 @@
 ROW_M, ROW_L, ROW_S, ROW_NK, ROW_NV, ROWS_C = 64, 66, 68, 70, 71, 72
 
 
-def project(tok_ref, gain_ref, wq_ref, wk_ref, wv_ref, out_ref):
+def project(tok_hbm, gain_hbm, wq_hbm, wk_hbm, wv_hbm, out_ref, tok_ref, gain_ref, wq_ref, wk_ref, wv_ref, sems):
+    copies = [
+        pltpu.make_async_copy(src, dst, sems.at[i])
+        for i, (src, dst) in enumerate(
+            [(tok_hbm, tok_ref), (gain_hbm, gain_ref), (wq_hbm, wq_ref), (wk_hbm, wk_ref), (wv_hbm, wv_ref)]
+        )
+    ]
+    for c in copies:
+        c.start()
+    for c in copies:
+        c.wait()
     peers = out_ref.shape[0]
     x = tok_ref[...].astype(jnp.float32)
     seqs = x.shape[0]
@@ -134,6 +144,10 @@
     for h in range(8):
         nk_ref[:, h * 128 : (h + 1) * 128] = nk[h * seqs : (h + 1) * seqs].astype(jnp.bfloat16)
         nv_ref[:, h * 128 : (h + 1) * 128] = nv[h * seqs : (h + 1) * seqs].astype(jnp.bfloat16)
+    sub = lax.broadcasted_iota(jnp.int32, (8, 128), 0)
+    lam = jnp.zeros((8, 128), jnp.float32)
+    for h in range(8):
+        lam = jnp.where(sub == h, lam_ref[h], lam)
     for b in range(seqs):
         maps = []
         fresh_v = v_scr[pl.ds(b, 8, stride=seqs), :]
@@ -143,15 +157,15 @@
             for j in range(peers):
                 acc = acc + scale[r : r + 8, j : j + 1] * got_ref[j, r : r + 8, :].astype(jnp.float32)
             maps.append(acc)
-        mixed = maps[0] - lam_ref[...] * maps[1]
+        mixed = maps[0] - lam * maps[1]
         mean = jnp.mean(mixed * mixed, axis=1, keepdims=True)
         head_scr[b * 8 : b * 8 + 8, :] = mixed * lax.rsqrt(mean + EPS) * gain_ref[...]
     heads = jnp.concatenate(
         [head_scr[pl.ds(h, seqs, stride=8), :] for h in range(8)], axis=1
     ).astype(jnp.bfloat16)
-    part_ref[...] = jnp.dot(heads, wo_ref[...], preferred_element_type=jnp.float32).astype(
-        jnp.bfloat16
-    )
+    part_ref[...] = lax.dot_general(
+        heads, wo_ref[...], (((1,), (1,)), ((), ())), preferred_element_type=jnp.float32
+    ).astype(jnp.bfloat16)
 
 
 VM = pl.BlockSpec(memory_space=pltpu.VMEM)
@@ -170,10 +184,20 @@
     sent = pl.pallas_call(
         project,
         out_shape=jax.ShapeDtypeStruct((peers, ROWS_A, 128), jnp.float32),
-        in_specs=[VM] * 5,
+        in_specs=[pl.BlockSpec(memory_space=pltpu.HBM)] * 5,
         out_specs=VM,
+        scratch_shapes=[
+            pltpu.VMEM(tokens.shape, jnp.bfloat16),
+            pltpu.VMEM((1, norm_gain.shape[0]), jnp.float32),
+            pltpu.VMEM(w_query.shape, jnp.bfloat16),
+            pltpu.VMEM(w_query.shape, jnp.bfloat16),
+            pltpu.VMEM(w_query.shape, jnp.bfloat16),
+            pltpu.SemaphoreType.DMA((5,)),
+        ],
         name="project",
-    )(tokens, norm_gain.reshape(1, -1), w_query, w_key, w_value)
+        cost_estimate=pl.CostEstimate(flops=5_000_000_000, bytes_accessed=30_000_000, transcendentals=0),
+        compiler_params=pltpu.CompilerParams(vmem_limit_bytes=8 << 20),
+    )(*(pltpu.with_memory_space_constraint(a, pltpu.HBM) for a in (tokens, norm_gain.reshape(1, -1), w_query, w_key, w_value)))
     got = exchange(sent)
     sent = pl.pallas_call(
         attend,
@@ -185,6 +209,7 @@
             pltpu.VMEM((64, 128), jnp.float32),
         ],
         name="attend",
+        compiler_params=pltpu.CompilerParams(vmem_limit_bytes=24 << 20),
     )(
         got,
         key_cache.reshape(seqs, span * heads, width),
@@ -199,18 +224,19 @@
             jax.ShapeDtypeStruct((seqs, heads * width), jnp.bfloat16),
             jax.ShapeDtypeStruct((seqs, heads * width), jnp.bfloat16),
         ),
-        in_specs=[VM] * 4,
+        in_specs=[VM, SM, VM, VM],
         out_specs=(VM, VM, VM),
         scratch_shapes=[
             pltpu.VMEM((32, 128), jnp.float32),
             pltpu.VMEM((32, 128), jnp.float32),
         ],
         name="merge",
+        compiler_params=pltpu.CompilerParams(vmem_limit_bytes=8 << 20),
     )(
         got,
-        jnp.broadcast_to(lam[:, None], (heads, 128)),
+        lam,
         head_gain.reshape(1, -1),
-        w_output,
+        w_output.T,
     )
     both = lax.all_gather(part, "tp")
     attended = jnp.sum(both.astype(jnp.float32), axis=0).astype(jnp.bfloat16)

time: 72.5 us -> 65.8 us (0.908)
  blocking collectives: 36 us -> 57.7 us
  waiting for transfers between devices: 15.8 us -> 0 us
  starting transfers between devices: 5.54 us -> 0 us
  Pallas kernels: 12 us -> 6.68 us
  local copies, waits for them, and re-layouts: 1.67 us -> 0.03 us
    all_to_all x1 -> x2, blocking collectives: 30.8 us -> 52.7 us  [exchange(): return lax.all_to_all(array, 'kv', split_axis=0, concat_axis=0, tiled=True)]
    all_to_all x1 -> x0, waiting for transfers between devices: 15.8 us -> none  [exchange(): return lax.all_to_all(array, 'kv', split_axis=0, concat_axis=0, tiled=True)]
    all_to_all x1 -> x0, starting transfers between devices: 5.54 us -> none  [exchange(): return lax.all_to_all(array, 'kv', split_axis=0, concat_axis=0, tiled=True)]
    pallas_call x1, Pallas kernels: 7.19 us -> 3.22 us  [per_device(): pl.pallas_call(attend, out_shape=jax.ShapeDtypeStruct((peers, ROWS_C, 128...]
    unnamed x7 -> x12, local copies, waits for them, and re-layouts: 0.91 us -> 0.03 us
    broadcast_in_dim x1 -> x0, local copies, waits for them, and re-layouts: 0.76 us -> none  [per_device(): jnp.broadcast_to(lam[:, None], (heads, 128))]
  transfers between devices with their start and end apart: 1 -> 0, of which waited for: 1 -> 0; matrix products, arithmetic and copies ran while one was open for 1% -> 0% of each run, Pallas kernels for 0% -> 0%
where the time goes in v2:
time: 65.8 us; the launch traced here: 65.7 us
  blocking collectives  57.7 us (88%)
  Pallas kernels  6.68 us (10%)
  between operations  0.71 us (1%)
    all_to_all x2, blocking collectives, exchange(): return lax.all_to_all(array, 'kv', split_axis=0, concat_axis=0, tiled=True)  52.7 us
    all_gather x1, blocking collectives, per_device(): both = lax.all_gather(part, 'tp')  4.97 us
    pallas_call x1, Pallas kernels, per_device(): pl.pallas_call(attend, out_shape=jax.ShapeDtypeStruct((peers, ROWS_C, 128...  3.22 us
    pallas_call x1, Pallas kernels, per_device(): pl.pallas_call(merge, out_shape=(jax.ShapeDtypeStruct((seqs, w_output.sha...  2.03 us
    pallas_call x1, Pallas kernels, per_device(): pl.pallas_call(project, out_shape=jax.ShapeDtypeStruct((peers, ROWS_A, 12...  1.43 us

profile of v2, /device:TPU:1, one launch (start us, length us, event | category | flops | bytes accessed | tf_op | source)
XLA Modules:
  0.0 65.7 jit_solution(14096835869240389931)
XLA Ops:
  0.6 0.0 copy-start
  0.6 0.0 copy-start.1
  0.7 0.0 copy-start.3
  0.7 1.4 %project.1 = f32[32,40,128]{2,1,0:T(8,128)S(1)} custom-call(bf16[4,64]{1,0:T(4,128)(2,1)} %tok_hbm.1, f32[1,64]{1,0:T(1,128)} %bitcast.11, bf16[64,1024]{1,0:T(8,128)(2,1)} %wq_hbm.1, bf16[64,1024]{1,0:T(8,128)(2,1)} %wk_hbm.1, bf16[64,1024]{1,0:T(8,128)(2,1)} %wv_hbm.1), custom_call_target="tpu_custom_call" | custom-call | flops 5000000000 | bytes 30000000 | tf_op jit(solution)/shard_map/project/pallas_call | solution.py:184
  2.1 30.8 %all_to_all.10.got_ref = f32[32,40,128]{2,1,0:T(8,128)S(1)} all-to-all(f32[32,40,128]{2,1,0:T(8,128)S(1)} %project.1), channel_id=1, replica_groups=mesh['dp'=4,'kv'=32,'tp'=2] {'kv'}, dimensions={0} | all-to-all | bytes 1310720 | tf_op jit(solution)/shard_map/all_to_all | solution.py:176
  32.9 0.0 copy-done
  32.9 0.0 copy-done.1
  32.9 0.0 copy-done.3
  32.9 0.0 copy-start.2
  32.9 0.0 copy-start.4
  32.9 0.0 copy-start.5
  32.9 3.2 %attend.1 = bf16[32,72,128]{2,1,0:T(8,128)(2,1)S(1)} custom-call(f32[32,40,128]{2,1,0:T(8,128)S(1)} %all_to_all.10.got_ref, bf16[4,4096,128]{2,1,0:T(8,128)(2,1)S(1)} %bitcast.6, bf16[4,4096,128]{2,1,0:T(8,128)(2,1)S(1)} %bitcast.7, s32[4]{0:T(128)S(1)} %copy-done.3), custom_call_target="tpu_custom_call" | custom-call | tf_op jit(solution)/shard_map/attend/pallas_call | solution.py:202
  36.1 21.9 %all_to_all.11.got_ref = bf16[32,72,128]{2,1,0:T(8,128)(2,1)S(1)} all-to-all(bf16[32,72,128]{2,1,0:T(8,128)(2,1)S(1)} %attend.1), channel_id=1, replica_groups=mesh['dp'=4,'kv'=32,'tp'=2] {'kv'}, dimensions={0} | all-to-all | bytes 1179648 | tf_op jit(solution)/shard_map/all_to_all | solution.py:176
  58.1 0.0 copy-done.2
  58.1 0.0 copy-done.4
  58.1 0.0 copy-done.5
  58.1 2.0 %merge.1 = (bf16[4,64]{1,0:T(4,128)(2,1)S(1)}, bf16[4,1024]{1,0:T(4,128)(2,1)}, bf16[4,1024]{1,0:T(4,128)(2,1)}) custom-call(bf16[32,72,128]{2,1,0:T(8,128)(2,1)S(1)} %all_to_all.11.got_ref, f32[8]{0:T(128)S(1)} %copy-done.4, f32[1,128]{1,0:T(1,128)S(1)} %bitcast.10, bf16[64,1024]{1,0:T(8,128)(2,1)S(1)} %bitcast.8), custom_call_target="tpu_custom_call" | custom-call | tf_op jit(solution)/shard_map/merge/pallas_call | solution.py:220
  60.1 5.0 %all-gather.1 = bf16[2,4,64]{2,1,0:T(4,128)(2,1)S(1)} all-gather(bf16[1,4,64]{2,1,0:T(4,128)(2,1)S(1)} %bitcast.9), channel_id=2, replica_groups=mesh['dp'=4,'kv'=32,'tp'=2] {'tp'}, dimensions={0}, use_global_device_ids=true | all-gather | bytes 1536 | tf_op jit(solution)/shard_map/all_gather | solution.py:241
  65.1 0.6 reduce_sum.12
Async XLA Ops:
  0.6 32.2 %copy-start = (bf16[4,512,8,128]{3,2,1,0:T(8,128)(2,1)S(1)}, bf16[4,512,8,128]{3,2,1,0:T(8,128)(2,1)}, u32[]{:S(2)}) copy-start(bf16[4,512,8,128]{3,2,1,0:T(8,128)(2,1)} %param.17) | copy-start | bytes 12582916
  0.6 32.2 %copy-start.1 = (bf16[4,512,8,128]{3,2,1,0:T(8,128)(2,1)S(1)}, bf16[4,512,8,128]{3,2,1,0:T(8,128)(2,1)}, u32[]{:S(2)}) copy-start(bf16[4,512,8,128]{3,2,1,0:T(8,128)(2,1)} %param.18) | copy-start | bytes 12582916
  0.7 32.2 %copy-start.3 = (s32[4]{0:T(128)S(1)}, s32[4]{0:T(128)}, u32[]{:S(2)}) copy-start(s32[4]{0:T(128)} %len_ref.1) | copy-start | bytes 52
  32.9 25.2 %copy-start.2 = (bf16[1024,64]{0,1:T(8,128)(2,1)S(1)}, bf16[1024,64]{0,1:T(8,128)(2,1)}, u32[]{:S(2)}) copy-start(bf16[1024,64]{0,1:T(8,128)(2,1)} %param.16) | copy-start | bytes 393220
  32.9 25.2 %copy-start.4 = (f32[8]{0:T(128)S(1)}, f32[8]{0:T(128)}, u32[]{:S(2)}) copy-start(f32[8]{0:T(128)} %lam_ref.1) | copy-start | bytes 100
  32.9 25.2 %copy-start.5 = (f32[128]{0:T(128)S(1)}, f32[128]{0:T(128)}, u32[]{:S(2)}) copy-start(f32[128]{0:T(128)} %param.21) | copy-start | bytes 1540

commit v3 on v2

--- a/solution.py
+++ b/solution.py
@@ -12,8 +12,12 @@
 EPS = 1e-6
 NEG = -1e30
 
-ROW_K, ROW_V, ROW_SQ, ROWS_A = 32, 33, 36, 40
+ROWS_A, BITS = 40, 14.5
 ROW_M, ROW_L, ROW_S, ROW_NK, ROW_NV, ROWS_C = 64, 66, 68, 70, 71, 72
+
+
+def exponent(a):
+    return jnp.ceil(jnp.log2(jnp.maximum(a, 1e-30)))
 
 
 def project(tok_hbm, gain_hbm, wq_hbm, wk_hbm, wv_hbm, out_ref, tok_ref, gain_ref, wq_ref, wk_ref, wv_ref, sems):
@@ -36,15 +40,34 @@
 
     def rows(w_ref):
         y = jnp.dot(scaled, w_ref[...], preferred_element_type=jnp.float32)
-        return jnp.concatenate([y[:, h * 128 : (h + 1) * 128] for h in range(heads)], axis=0)
-
-    q, k, v = rows(wq_ref), rows(wk_ref), rows(wv_ref)
-    sq = jnp.broadcast_to(squares, (seqs, 128))
+        e = exponent(jnp.max(jnp.abs(y), axis=1, keepdims=True))
+        y = jnp.round(y * jnp.exp2(BITS - e))
+        return jnp.concatenate([y[:, h * 128 : (h + 1) * 128] for h in range(heads)], axis=0), e
+
+    (q, qe), (k, ke), (v, ve) = rows(wq_ref), rows(wk_ref), rows(wv_ref)
+    se = exponent(squares)
+    size = squares * jnp.exp2(BITS - se)
+    whole = jnp.floor(size)
+    rest = jnp.round((size - whole) * 2.0**14)
+    lane = lax.broadcasted_iota(jnp.int32, (seqs, 128), 1)
+    meta = jnp.where(
+        lane == 0, qe, jnp.where(lane == 1, se, jnp.where(lane == 2, whole, rest))
+    )
+    q = q.astype(jnp.int32).astype(jnp.int16)
     for j in range(peers):
+        b = j % seqs
+        tile = jnp.concatenate(
+            [
+                k[j : j + 1],
+                v[j : j + 1],
+                jnp.broadcast_to(ke[b : b + 1], (1, 128)),
+                jnp.broadcast_to(ve[b : b + 1], (1, 128)),
+                meta,
+            ],
+            axis=0,
+        )
         out_ref[j, 0:32, :] = q
-        out_ref[j, ROW_K : ROW_K + 1, :] = k[j : j + 1, :]
-        out_ref[j, ROW_V : ROW_V + 1, :] = v[j : j + 1, :]
-        out_ref[j, ROW_SQ : ROW_SQ + seqs, :] = sq
+        out_ref[j, 32:40, :] = tile.astype(jnp.int32).astype(jnp.int16)
 
 
 def two_pieces(a):
@@ -58,18 +81,28 @@
     width = key_ref.shape[1]
     span = width // 8
     me = lax.axis_index("kv")
-    total = got_ref[0]
-    for j in range(1, peers):
-        total = total + got_ref[j]
-    inv = lax.rsqrt(total[ROW_SQ : ROW_SQ + seqs] / D + EPS)
+    total = [jnp.zeros((8, 128), jnp.float32)] * 4
+    own = jnp.zeros((8, 128), jnp.float32)
+    squares = jnp.zeros((8, 128), jnp.float32)
+    for j in range(peers):
+        got = got_ref[j].astype(jnp.int32).astype(jnp.float32)
+        tile = got[32:40]
+        unit = jnp.exp2(tile - BITS)
+        units = jnp.concatenate([unit[4:8, 0:1]] * 2, axis=0)
+        total = [t + got[i * 8 : i * 8 + 8] * units for i, t in enumerate(total)]
+        own = own + tile * pltpu.roll(unit, 6, 0)
+        size = tile + pltpu.roll(tile, 127, 1) * 2.0**-14
+        squares = squares + size * pltpu.roll(unit, 1, 1)
+    total = jnp.concatenate(total, axis=0)
+    inv = lax.rsqrt(jnp.broadcast_to(squares[4:8, 2:3], (4, 128)) / D + EPS)
     inv8 = jnp.concatenate([inv, inv], axis=0)
     inv32 = jnp.concatenate([inv8] * 4, axis=0)
-    q = (total[0:32] * inv32).astype(jnp.bfloat16).astype(jnp.float32)
+    q = (total * inv32).astype(jnp.bfloat16).astype(jnp.float32)
     q_scr[...] = q
     seq_id = lax.broadcasted_iota(jnp.int32, (seqs, 128), 0)
     mine = jnp.sum(jnp.where(seq_id == lax.rem(me, seqs), inv, 0.0), axis=0, keepdims=True)
-    nk = (total[ROW_K : ROW_K + 1] * mine).astype(jnp.bfloat16)
-    nv = (total[ROW_V : ROW_V + 1] * mine).astype(jnp.bfloat16)
+    nk = (own[0:1] * mine).astype(jnp.bfloat16)
+    nv = (own[1:2] * mine).astype(jnp.bfloat16)
     lane = lax.broadcasted_iota(jnp.int32, (8, 128), 1)
     sub = lax.broadcasted_iota(jnp.int32, (8, 128), 0)
     lane1 = lax.broadcasted_iota(jnp.int32, (1, 128), 1)
@@ -183,7 +216,7 @@
     seqs, span, heads, width = key_cache.shape
     sent = pl.pallas_call(
         project,
-        out_shape=jax.ShapeDtypeStruct((peers, ROWS_A, 128), jnp.float32),
+        out_shape=jax.ShapeDtypeStruct((peers, ROWS_A, 128), jnp.int16),
         in_specs=[pl.BlockSpec(memory_space=pltpu.HBM)] * 5,
         out_specs=VM,
         scratch_shapes=[

time: 65.8 us -> 59.3 us (0.901)
  blocking collectives: 57.7 us -> 50.8 us
    all_to_all x2, blocking collectives: 52.7 us -> 46 us  [exchange(): return lax.all_to_all(array, 'kv', split_axis=0, concat_axis=0, tiled=True)]
where the time goes in v3:
time: 59.3 us; the launch traced here: 59.1 us
  blocking collectives  50.8 us (86%)
  Pallas kernels  7 us (12%)
  between operations  0.71 us (1%)
    all_to_all x2, blocking collectives, exchange(): return lax.all_to_all(array, 'kv', split_axis=0, concat_axis=0, tiled=True)  46 us
    all_gather x1, blocking collectives, per_device(): both = lax.all_gather(part, 'tp')  4.86 us
    pallas_call x1, Pallas kernels, per_device(): pl.pallas_call(attend, out_shape=jax.ShapeDtypeStruct((peers, ROWS_C, 128...  3.38 us
    pallas_call x1, Pallas kernels, per_device(): pl.pallas_call(merge, out_shape=(jax.ShapeDtypeStruct((seqs, w_output.sha...  2.03 us
    pallas_call x1, Pallas kernels, per_device(): pl.pallas_call(project, out_shape=jax.ShapeDtypeStruct((peers, ROWS_A, 12...  1.59 us

profile of v3, /device:TPU:1, one launch (start us, length us, event | category | flops | bytes accessed | tf_op | source)
XLA Modules:
  0.0 59.1 jit_solution(2208666839678252583)
XLA Ops:
  0.6 0.0 copy-start
  0.6 0.0 copy-start.1
  0.7 0.0 copy-start.3
  0.7 1.6 %project.1 = s16[32,40,128]{2,1,0:T(8,128)(2,1)S(1)} custom-call(bf16[4,64]{1,0:T(4,128)(2,1)} %tok_hbm.1, f32[1,64]{1,0:T(1,128)} %bitcast.11, bf16[64,1024]{1,0:T(8,128)(2,1)} %wq_hbm.1, bf16[64,1024]{1,0:T(8,128)(2,1)} %wk_hbm.1, bf16[64,1024]{1,0:T(8,128)(2,1)} %wv_hbm.1), custom_call_target="tpu_custom_call" | custom-call | flops 5000000000 | bytes 30000000 | tf_op jit(solution)/shard_map/project/pallas_call | solution.py:217
  2.3 24.8 %all_to_all.10.got_ref = s16[32,40,128]{2,1,0:T(8,128)(2,1)S(1)} all-to-all(s16[32,40,128]{2,1,0:T(8,128)(2,1)S(1)} %project.1), channel_id=1, replica_groups=mesh['dp'=4,'kv'=32,'tp'=2] {'kv'}, dimensions={0} | all-to-all | bytes 655360 | tf_op jit(solution)/shard_map/all_to_all | solution.py:209
  27.1 0.0 copy-done
  27.1 0.0 copy-done.1
  27.1 0.0 copy-done.3
  27.1 0.0 copy-start.2
  27.1 0.0 copy-start.4
  27.1 0.0 copy-start.5
  27.1 3.4 %attend.1 = bf16[32,72,128]{2,1,0:T(8,128)(2,1)S(1)} custom-call(s16[32,40,128]{2,1,0:T(8,128)(2,1)S(1)} %all_to_all.10.got_ref, bf16[4,4096,128]{2,1,0:T(8,128)(2,1)S(1)} %bitcast.6, bf16[4,4096,128]{2,1,0:T(8,128)(2,1)S(1)} %bitcast.7, s32[4]{0:T(128)S(1)} %copy-done.3), custom_call_target="tpu_custom_call" | custom-call | tf_op jit(solution)/shard_map/attend/pallas_call | solution.py:235
  30.5 21.2 %all_to_all.11.got_ref = bf16[32,72,128]{2,1,0:T(8,128)(2,1)S(1)} all-to-all(bf16[32,72,128]{2,1,0:T(8,128)(2,1)S(1)} %attend.1), channel_id=1, replica_groups=mesh['dp'=4,'kv'=32,'tp'=2] {'kv'}, dimensions={0} | all-to-all | bytes 1179648 | tf_op jit(solution)/shard_map/all_to_all | solution.py:209
  51.7 0.0 copy-done.2
  51.7 0.0 copy-done.4
  51.7 0.0 copy-done.5
  51.7 2.0 %merge.1 = (bf16[4,64]{1,0:T(4,128)(2,1)S(1)}, bf16[4,1024]{1,0:T(4,128)(2,1)}, bf16[4,1024]{1,0:T(4,128)(2,1)}) custom-call(bf16[32,72,128]{2,1,0:T(8,128)(2,1)S(1)} %all_to_all.11.got_ref, f32[8]{0:T(128)S(1)} %copy-done.4, f32[1,128]{1,0:T(1,128)S(1)} %bitcast.10, bf16[64,1024]{1,0:T(8,128)(2,1)S(1)} %bitcast.8), custom_call_target="tpu_custom_call" | custom-call | tf_op jit(solution)/shard_map/merge/pallas_call | solution.py:253
  53.7 4.9 %all-gather.1 = bf16[2,4,64]{2,1,0:T(4,128)(2,1)S(1)} all-gather(bf16[1,4,64]{2,1,0:T(4,128)(2,1)S(1)} %bitcast.9), channel_id=2, replica_groups=mesh['dp'=4,'kv'=32,'tp'=2] {'tp'}, dimensions={0}, use_global_device_ids=true | all-gather | bytes 1536 | tf_op jit(solution)/shard_map/all_gather | solution.py:274
  58.5 0.6 reduce_sum.12
Async XLA Ops:
  0.6 26.4 %copy-start = (bf16[4,512,8,128]{3,2,1,0:T(8,128)(2,1)S(1)}, bf16[4,512,8,128]{3,2,1,0:T(8,128)(2,1)}, u32[]{:S(2)}) copy-start(bf16[4,512,8,128]{3,2,1,0:T(8,128)(2,1)} %param.17) | copy-start | bytes 12582916
  0.6 26.4 %copy-start.1 = (bf16[4,512,8,128]{3,2,1,0:T(8,128)(2,1)S(1)}, bf16[4,512,8,128]{3,2,1,0:T(8,128)(2,1)}, u32[]{:S(2)}) copy-start(bf16[4,512,8,128]{3,2,1,0:T(8,128)(2,1)} %param.18) | copy-start | bytes 12582916
  0.7 26.4 %copy-start.3 = (s32[4]{0:T(128)S(1)}, s32[4]{0:T(128)}, u32[]{:S(2)}) copy-start(s32[4]{0:T(128)} %len_ref.1) | copy-start | bytes 52
  27.1 24.6 %copy-start.2 = (bf16[1024,64]{0,1:T(8,128)(2,1)S(1)}, bf16[1024,64]{0,1:T(8,128)(2,1)}, u32[]{:S(2)}) copy-start(bf16[1024,64]{0,1:T(8,128)(2,1)} %param.16) | copy-start | bytes 393220
  27.1 24.6 %copy-start.4 = (f32[8]{0:T(128)S(1)}, f32[8]{0:T(128)}, u32[]{:S(2)}) copy-start(f32[8]{0:T(128)} %lam_ref.1) | copy-start | bytes 100
  27.1 24.6 %copy-start.5 = (f32[128]{0:T(128)S(1)}, f32[128]{0:T(128)}, u32[]{:S(2)}) copy-start(f32[128]{0:T(128)} %param.21) | copy-start | bytes 1540

commit v4 on v3

--- a/solution.py
+++ b/solution.py
@@ -1,10 +1,9 @@
-import functools
-
 import jax
 import jax.numpy as jnp
 from jax import lax
 from jax.experimental import pallas as pl
 from jax.experimental.pallas import tpu as pltpu
+from jax.sharding import Mesh
 from jax.sharding import PartitionSpec as P
 
 D = 2048
@@ -14,7 +13,7 @@
 
 ROWS_A, BITS = 40, 14.5
 ROW_M, ROW_L, ROW_S, ROW_NK, ROW_NV, ROWS_C = 64, 66, 68, 70, 71, 72
-
+ROW_NKS, ROW_NVS, ROWS_E = 72, 80, 88
 
 def exponent(a):
     return jnp.ceil(jnp.log2(jnp.maximum(a, 1e-30)))
@@ -80,7 +79,7 @@
     seqs = key_ref.shape[0]
     width = key_ref.shape[1]
     span = width // 8
-    me = lax.axis_index("kv")
+    me = lax.axis_index("kv_0") * lax.axis_size("kv_1") + lax.axis_index("kv_1")
     total = [jnp.zeros((8, 128), jnp.float32)] * 4
     own = jnp.zeros((8, 128), jnp.float32)
     squares = jnp.zeros((8, 128), jnp.float32)
@@ -144,53 +143,76 @@
         [turned[0:4], shi, slo, nk.astype(jnp.float32), nv.astype(jnp.float32)], axis=0
     )
     packed = jnp.concatenate(accs + [tail], axis=0).astype(jnp.bfloat16)
-    for j in range(peers):
+    for j in range(out_ref.shape[0]):
         out_ref[j] = packed
 
 
-def merge(got_ref, lam_ref, gain_ref, wo_ref, part_ref, nk_ref, nv_ref, head_scr, v_scr):
+def tails(got_ref):
     peers = got_ref.shape[0]
-    seqs = nk_ref.shape[0]
-
-    def row(r):
-        return jnp.concatenate(
-            [got_ref[j, ROW_M:ROWS_C, :].astype(jnp.float32)[r - ROW_M : r - ROW_M + 1] for j in range(peers)],
-            axis=0,
-        )
-
+    tiles = [got_ref[j, ROW_M : ROW_M + 8, :].astype(jnp.float32) for j in range(peers)]
+    return lambda r: jnp.concatenate([t[r - ROW_M : r - ROW_M + 1] for t in tiles], axis=0)
+
+
+def columns(rows):
+    used = sum(r.shape[0] for r in rows)
+    return jnp.concatenate(rows + [jnp.zeros((128 - used, 128), jnp.float32)], axis=0).T
+
+
+def weighted(got_ref, scale, r):
+    acc = scale[r : r + 8, 0:1] * got_ref[0, r : r + 8, :].astype(jnp.float32)
+    for j in range(1, got_ref.shape[0]):
+        acc = acc + scale[r : r + 8, j : j + 1] * got_ref[j, r : r + 8, :].astype(jnp.float32)
+    return acc
+
+
+def merge_first(got_ref, out_ref):
+    peers = got_ref.shape[0]
+    row = tails(got_ref)
     top = row(ROW_M) + row(ROW_M + 1)
     part = row(ROW_L) + row(ROW_L + 1)
     snew = row(ROW_S) + row(ROW_S + 1)
-    peak = jnp.maximum(
-        jnp.max(top, axis=0, keepdims=True), jnp.max(snew, axis=0, keepdims=True)
-    )
+    peak = jnp.max(jnp.maximum(top, snew), axis=0, keepdims=True)
     factor = jnp.exp(top - peak)
-    fresh = jnp.sum(jnp.exp(snew - peak), axis=0, keepdims=True)
+    fresh = jnp.sum(jnp.where(snew > 0.5 * NEG, jnp.exp(snew - peak), 0.0), axis=0, keepdims=True)
     total = jnp.sum(part * factor, axis=0, keepdims=True) + fresh
-    scale = jnp.concatenate(
-        [factor / total, jnp.broadcast_to(fresh / total, (8, 128)), jnp.zeros((88, 128), jnp.float32)],
-        axis=0,
-    ).T
-    nk = row(ROW_NK)
-    nv = row(ROW_NV)
-    v_scr[...] = nv
+    scale = columns([factor, jnp.broadcast_to(fresh, (8, 128))])
+    nk, nv = row(ROW_NK), row(ROW_NV)
+    accs = []
+    for r in range(0, ROW_M, 8):
+        accs.append(weighted(got_ref, scale, r) + scale[r : r + 8, peers : peers + 1] * nv)
+    tail = jnp.concatenate(
+        [*two_pieces(peak), *two_pieces(total), jnp.zeros((4, 128), jnp.float32)], axis=0
+    )
+    packed = jnp.concatenate(accs + [tail, nk, nv], axis=0).astype(jnp.bfloat16)
+    for j in range(out_ref.shape[0]):
+        out_ref[j] = packed
+
+
+def merge_last(got_ref, lam_ref, gain_ref, wo_ref, part_ref, nk_out, nv_out, nk_ref, nv_ref, head_scr, sems):
+    seqs = nk_ref.shape[0]
     for h in range(8):
-        nk_ref[:, h * 128 : (h + 1) * 128] = nk[h * seqs : (h + 1) * seqs].astype(jnp.bfloat16)
-        nv_ref[:, h * 128 : (h + 1) * 128] = nv[h * seqs : (h + 1) * seqs].astype(jnp.bfloat16)
+        for dst, r in ((nk_ref, ROW_NKS), (nv_ref, ROW_NVS)):
+            dst[:, h * 128 : (h + 1) * 128] = jnp.concatenate(
+                [got_ref[b, r : r + 8, :].astype(jnp.float32)[h : h + 1] for b in range(seqs)], axis=0
+            ).astype(jnp.bfloat16)
+    copies = [
+        pltpu.make_async_copy(nk_ref, nk_out, sems.at[0]),
+        pltpu.make_async_copy(nv_ref, nv_out, sems.at[1]),
+    ]
+    for c in copies:
+        c.start()
+    row = tails(got_ref)
+    top = row(ROW_M) + row(ROW_M + 1)
+    part = row(ROW_L) + row(ROW_L + 1)
+    factor = jnp.exp(top - jnp.max(top, axis=0, keepdims=True))
+    total = jnp.sum(part * factor, axis=0, keepdims=True)
+    scale = columns([factor / total])
     sub = lax.broadcasted_iota(jnp.int32, (8, 128), 0)
     lam = jnp.zeros((8, 128), jnp.float32)
     for h in range(8):
         lam = jnp.where(sub == h, lam_ref[h], lam)
     for b in range(seqs):
-        maps = []
-        fresh_v = v_scr[pl.ds(b, 8, stride=seqs), :]
-        for m in range(2):
-            r = b * 16 + m * 8
-            acc = scale[r : r + 8, peers : peers + 1] * fresh_v
-            for j in range(peers):
-                acc = acc + scale[r : r + 8, j : j + 1] * got_ref[j, r : r + 8, :].astype(jnp.float32)
-            maps.append(acc)
-        mixed = maps[0] - lam * maps[1]
+        mixed = weighted(got_ref, scale, b * 16) - lam * weighted(got_ref, scale, b * 16 + 8)
         mean = jnp.mean(mixed * mixed, axis=1, keepdims=True)
         head_scr[b * 8 : b * 8 + 8, :] = mixed * lax.rsqrt(mean + EPS) * gain_ref[...]
     heads = jnp.concatenate(
@@ -199,20 +221,25 @@
     part_ref[...] = lax.dot_general(
         heads, wo_ref[...], (((1,), (1,)), ((), ())), preferred_element_type=jnp.float32
     ).astype(jnp.bfloat16)
+    for c in copies:
+        c.wait()
 
 
 VM = pl.BlockSpec(memory_space=pltpu.VMEM)
 SM = pl.BlockSpec(memory_space=pltpu.SMEM)
 
 
-def exchange(array):
-    return lax.all_to_all(array, "kv", split_axis=0, concat_axis=0, tiled=True)
+KV = ("kv_0", "kv_1")
+
+
+def exchange(array, axis):
+    return lax.all_to_all(array, axis, split_axis=0, concat_axis=0, tiled=True)
 
 
 def per_device(
     tokens, norm_gain, w_query, w_key, w_value, w_output, key_cache, value_cache, lengths, lam, head_gain
 ):
-    peers = lax.axis_size("kv")
+    peers = lax.axis_size(KV)
     seqs, span, heads, width = key_cache.shape
     sent = pl.pallas_call(
         project,
@@ -231,10 +258,10 @@
         cost_estimate=pl.CostEstimate(flops=5_000_000_000, bytes_accessed=30_000_000, transcendentals=0),
         compiler_params=pltpu.CompilerParams(vmem_limit_bytes=8 << 20),
     )(*(pltpu.with_memory_space_constraint(a, pltpu.HBM) for a in (tokens, norm_gain.reshape(1, -1), w_query, w_key, w_value)))
-    got = exchange(sent)
+    got = exchange(sent, KV)
     sent = pl.pallas_call(
         attend,
-        out_shape=jax.ShapeDtypeStruct((peers, ROWS_C, 128), jnp.bfloat16),
+        out_shape=jax.ShapeDtypeStruct((lax.axis_size("kv_0"), ROWS_C, 128), jnp.bfloat16),
         in_specs=[VM, VM, VM, SM],
         out_specs=VM,
         scratch_shapes=[
@@ -249,50 +276,56 @@
         value_cache.reshape(seqs, span * heads, width),
         lengths,
     )
-    got = exchange(sent)
+    got = exchange(sent, "kv_0")
+    sent = pl.pallas_call(
+        merge_first,
+        out_shape=jax.ShapeDtypeStruct((lax.axis_size("kv_1"), ROWS_E, 128), jnp.bfloat16),
+        in_specs=[VM],
+        out_specs=VM,
+        name="merge_first",
+        compiler_params=pltpu.CompilerParams(vmem_limit_bytes=8 << 20),
+    )(got)
+    got = exchange(sent, "kv_1")
+    row = jax.ShapeDtypeStruct((seqs, heads * width), jnp.bfloat16)
     part, new_key, new_value = pl.pallas_call(
-        merge,
-        out_shape=(
-            jax.ShapeDtypeStruct((seqs, w_output.shape[1]), jnp.bfloat16),
-            jax.ShapeDtypeStruct((seqs, heads * width), jnp.bfloat16),
-            jax.ShapeDtypeStruct((seqs, heads * width), jnp.bfloat16),
-        ),
+        merge_last,
+        out_shape=(jax.ShapeDtypeStruct((seqs, w_output.shape[1]), jnp.bfloat16), row, row),
         in_specs=[VM, SM, VM, VM],
-        out_specs=(VM, VM, VM),
+        out_specs=(VM, pl.BlockSpec(memory_space=pltpu.HBM), pl.BlockSpec(memory_space=pltpu.HBM)),
         scratch_shapes=[
+            pltpu.VMEM(row.shape, row.dtype),
+            pltpu.VMEM(row.shape, row.dtype),
             pltpu.VMEM((32, 128), jnp.float32),
-            pltpu.VMEM((32, 128), jnp.float32),
+            pltpu.SemaphoreType.DMA((2,)),
         ],
-        name="merge",
+        name="merge_last",
         compiler_params=pltpu.CompilerParams(vmem_limit_bytes=8 << 20),
-    )(
-        got,
-        lam,
-        head_gain.reshape(1, -1),
-        w_output.T,
-    )
+    )(got, lam, head_gain.reshape(1, -1), w_output.T)
     both = lax.all_gather(part, "tp")
     attended = jnp.sum(both.astype(jnp.float32), axis=0).astype(jnp.bfloat16)
     return (attended, new_key, new_value)
 
 
 def solution(mesh):
+    split = Mesh(
+        mesh.devices.reshape(mesh.shape["dp"], 8, 4, mesh.shape["tp"]), ("dp", "kv_0", "kv_1", "tp")
+    )
     return jax.shard_map(
         per_device,
-        mesh=mesh,
+        mesh=split,
         in_specs=(
-            P("dp", "kv"),
-            P("kv"),
-            P("kv", "tp"),
-            P("kv", "tp"),
-            P("kv", "tp"),
-            P("tp", "kv"),
-            P("dp", "kv", "tp", None),
-            P("dp", "kv", "tp", None),
+            P("dp", KV),
+            P(KV),
+            P(KV, "tp"),
+            P(KV, "tp"),
+            P(KV, "tp"),
+            P("tp", KV),
+            P("dp", KV, "tp", None),
+            P("dp", KV, "tp", None),
             P("dp"),
             P("tp"),
             P(),
         ),
-        out_specs=(P("dp", "kv"), P("dp", "tp"), P("dp", "tp")),
+        out_specs=(P("dp", KV), P("dp", "tp"), P("dp", "tp")),
         check_vma=False,
     )

time: 59.3 us -> 57.2 us (0.965)
  blocking collectives: 50.8 us -> 48.9 us
    all_to_all x2 -> x3, blocking collectives: 46 us -> 43.1 us  [exchange(): return lax.all_to_all(array, axis, split_axis=0, concat_axis=0, tiled=True)]
    all_gather x1, blocking collectives: 4.86 us -> 5.78 us  [per_device(): both = lax.all_gather(part, 'tp')]
    pallas_call x2 -> x3, Pallas kernels: 5.41 us -> 5.18 us  [the longest x1 3.36 us: per_device(): pl.pallas_call(attend, out_shape=jax.ShapeDtypeStruct((lax.axis_size('kv_...]
where the time goes in v4:
time: 57.2 us; the launch traced here: 57 us
  blocking collectives  48.9 us (85%)
  Pallas kernels  6.77 us (12%)
  between operations  0.71 us (1%)
    all_to_all x3, blocking collectives, exchange(): return lax.all_to_all(array, axis, split_axis=0, concat_axis=0, tiled=True)  43.1 us
    all_gather x1, blocking collectives, per_device(): both = lax.all_gather(part, 'tp')  5.78 us
    pallas_call x1, Pallas kernels, per_device(): pl.pallas_call(attend, out_shape=jax.ShapeDtypeStruct((lax.axis_size('kv_...  3.36 us
    pallas_call x1, Pallas kernels, per_device(): pl.pallas_call(project, out_shape=jax.ShapeDtypeStruct((peers, ROWS_A, 12...  1.59 us
    pallas_call x1, Pallas kernels, per_device(): pl.pallas_call(merge_last, out_shape=(jax.ShapeDtypeStruct((seqs, w_outpu...  1.52 us

profile of v4, /device:TPU:1, one launch (start us, length us, event | category | flops | bytes accessed | tf_op | source)
XLA Modules:
  0.0 57.0 jit_solution(9852601740446836314)
XLA Ops:
  0.6 0.0 copy-start
  0.6 0.0 copy-start.1
  0.7 0.0 copy-start.3
  0.7 1.6 %project.1 = s16[32,40,128]{2,1,0:T(8,128)(2,1)S(1)} custom-call(bf16[4,64]{1,0:T(4,128)(2,1)} %tok_hbm.1, f32[1,64]{1,0:T(1,128)} %bitcast.11, bf16[64,1024]{1,0:T(8,128)(2,1)} %wq_hbm.1, bf16[64,1024]{1,0:T(8,128)(2,1)} %wk_hbm.1, bf16[64,1024]{1,0:T(8,128)(2,1)} %wv_hbm.1), custom_call_target="tpu_custom_call" | custom-call | flops 5000000000 | bytes 30000000 | tf_op jit(solution)/shard_map/project/pallas_call | solution.py:244
  2.3 24.8 %all_to_all.15.got_ref = s16[32,40,128]{2,1,0:T(8,128)(2,1)S(1)} all-to-all(s16[32,40,128]{2,1,0:T(8,128)(2,1)S(1)} %project.1), channel_id=1, replica_groups=mesh['dp'=4,'kv_0'=8,'kv_1'=4,'tp'=2] {'kv_0','kv_1'}, dimensions={0} | all-to-all | bytes 655360 | tf_op jit(solution)/shard_map/all_to_all | solution.py:236
  27.1 0.0 copy-done
  27.1 0.0 copy-done.1
  27.1 0.0 copy-done.3
  27.1 0.0 copy-start.2
  27.1 0.0 copy-start.4
  27.1 0.0 copy-start.5
  27.1 3.4 %attend.1 = bf16[8,72,128]{2,1,0:T(8,128)(2,1)S(1)} custom-call(s16[32,40,128]{2,1,0:T(8,128)(2,1)S(1)} %all_to_all.15.got_ref, bf16[4,4096,128]{2,1,0:T(8,128)(2,1)S(1)} %bitcast.6, bf16[4,4096,128]{2,1,0:T(8,128)(2,1)S(1)} %bitcast.7, s32[4]{0:T(128)S(1)} %copy-done.3), custom_call_target="tpu_custom_call" | custom-call | tf_op jit(solution)/shard_map/attend/pallas_call | solution.py:262
  30.5 11.0 %all_to_all.16.got_ref = bf16[8,72,128]{2,1,0:T(8,128)(2,1)S(1)} all-to-all(bf16[8,72,128]{2,1,0:T(8,128)(2,1)S(1)} %attend.1), channel_id=1, replica_groups=mesh['dp'=4,'kv_0'=8,'kv_1'=4,'tp'=2] {'kv_0'}, dimensions={0} | all-to-all | bytes 294912 | tf_op jit(solution)/shard_map/all_to_all | solution.py:236
  41.5 0.3 merge_first.1
  41.8 7.3 %all_to_all.17.got_ref = bf16[4,88,128]{2,1,0:T(8,128)(2,1)S(1)} all-to-all(bf16[4,88,128]{2,1,0:T(8,128)(2,1)S(1)} %merge_first.1), channel_id=1, replica_groups=mesh['dp'=4,'kv_0'=8,'kv_1'=4,'tp'=2] {'kv_1'}, dimensions={0} | all-to-all | bytes 180224 | tf_op jit(solution)/shard_map/all_to_all | solution.py:236
  49.1 0.0 copy-done.2
  49.1 0.0 copy-done.4
  49.1 0.0 copy-done.5
  49.1 1.5 %merge_last.1 = (bf16[4,64]{1,0:T(4,128)(2,1)S(1)}, bf16[4,1024]{1,0:T(4,128)(2,1)}, bf16[4,1024]{1,0:T(4,128)(2,1)}) custom-call(bf16[4,88,128]{2,1,0:T(8,128)(2,1)S(1)} %all_to_all.17.got_ref, f32[8]{0:T(128)S(1)} %copy-done.4, f32[1,128]{1,0:T(1,128)S(1)} %bitcast.10, bf16[64,1024]{1,0:T(8,128)(2,1)S(1)} %bitcast.8), custom_call_target="tpu_custom_call" | custom-call | tf_op jit(solution)/shard_map/merge_last/pallas_call | solution.py:290
  50.6 5.8 %all-gather.1 = bf16[2,4,64]{2,1,0:T(4,128)(2,1)S(1)} all-gather(bf16[1,4,64]{2,1,0:T(4,128)(2,1)S(1)} %bitcast.9), channel_id=2, replica_groups=mesh['dp'=4,'kv_0'=8,'kv_1'=4,'tp'=2] {'tp'}, dimensions={0}, use_global_device_ids=true | all-gather | bytes 1536 | tf_op jit(solution)/shard_map/all_gather | solution.py:304
  56.4 0.6 %reduce_sum.12 = bf16[4,64]{1,0:T(4,128)(2,1)} reduce(bf16[2,4,64]{2,1,0:T(4,128)(2,1)S(1)} %all-gather.1, bf16[]{:T(256)} %constant.2.clone.1), dimensions={0}, to_apply=%region_0.0 | reduce | flops 256 | bytes 1538 | tf_op jit(solution)/shard_map/reduce_sum | solution.py:305
Async XLA Ops:
  0.6 26.4 %copy-start = (bf16[4,512,8,128]{3,2,1,0:T(8,128)(2,1)S(1)}, bf16[4,512,8,128]{3,2,1,0:T(8,128)(2,1)}, u32[]{:S(2)}) copy-start(bf16[4,512,8,128]{3,2,1,0:T(8,128)(2,1)} %param.17) | copy-start | bytes 12582916
  0.6 26.4 %copy-start.1 = (bf16[4,512,8,128]{3,2,1,0:T(8,128)(2,1)S(1)}, bf16[4,512,8,128]{3,2,1,0:T(8,128)(2,1)}, u32[]{:S(2)}) copy-start(bf16[4,512,8,128]{3,2,1,0:T(8,128)(2,1)} %param.18) | copy-start | bytes 12582916
  0.7 26.4 %copy-start.3 = (s32[4]{0:T(128)S(1)}, s32[4]{0:T(128)}, u32[]{:S(2)}) copy-start(s32[4]{0:T(128)} %len_ref.1) | copy-start | bytes 52
  27.1 22.0 %copy-start.2 = (bf16[1024,64]{0,1:T(8,128)(2,1)S(1)}, bf16[1024,64]{0,1:T(8,128)(2,1)}, u32[]{:S(2)}) copy-start(bf16[1024,64]{0,1:T(8,128)(2,1)} %param.16) | copy-start | bytes 393220
  27.1 22.0 %copy-start.4 = (f32[8]{0:T(128)S(1)}, f32[8]{0:T(128)}, u32[]{:S(2)}) copy-start(f32[8]{0:T(128)} %lam_ref.1) | copy-start | bytes 100
  27.1 22.0 %copy-start.5 = (f32[128]{0:T(128)S(1)}, f32[128]{0:T(128)}, u32[]{:S(2)}) copy-start(f32[128]{0:T(128)} %param.21) | copy-start | bytes 1540

commit v5 on v4

--- a/solution.py
+++ b/solution.py
@@ -113,15 +113,17 @@
     own_head = lax.rem(lane, 8) == sub
     col = lax.broadcasted_iota(jnp.int32, (8, width), 1)
     own_head_wide = lax.rem(col, 8) == lax.broadcasted_iota(jnp.int32, (8, width), 0)
-    accs = []
-    for b in range(seqs):
+
+    def score(b):
         qb = q_scr[pl.ds(b, 8, stride=seqs), :] * HEAD_WIDTH**-0.5
         q1 = jnp.where(lane < HEAD_WIDTH, qb, 0.0)
         q2 = jnp.where(lane >= HEAD_WIDTH, qb, 0.0)
         q16 = jnp.concatenate([q1, q2], axis=0).astype(jnp.bfloat16)
-        s = lax.dot_general(
+        return lax.dot_general(
             q16, key_ref[b], (((1,), (1,)), ((), ())), preferred_element_type=jnp.float32
         )
+
+    def weigh(b, s):
         limit = (len_ref[b] - me * span) * 8
         live = jnp.logical_and(own_head_wide, col < limit)
         weights = []
@@ -135,8 +137,14 @@
             col_scr[r : r + 8, :] = jnp.where(
                 lane == 0, hi, jnp.where(lane == 1, lo, jnp.where(lane == 2, lhi, llo))
             )
-        w16 = jnp.concatenate(weights, axis=0).astype(jnp.bfloat16)
-        accs.append(jnp.dot(w16, val_ref[b], preferred_element_type=jnp.float32))
+        return jnp.concatenate(weights, axis=0).astype(jnp.bfloat16)
+
+    def values(b, w):
+        return jnp.dot(w, val_ref[b], preferred_element_type=jnp.float32)
+
+    scores = [score(b) for b in range(seqs)]
+    weights = [weigh(b, scores[b]) for b in range(seqs)]
+    accs = [values(b, weights[b]) for b in range(seqs)]
     turned = jnp.concatenate([col_scr[...], jnp.zeros_like(col_scr)], axis=0).T
     shi, slo = two_pieces(snew)
     tail = jnp.concatenate(
@@ -188,19 +196,17 @@
         out_ref[j] = packed
 
 
-def merge_last(got_ref, lam_ref, gain_ref, wo_ref, part_ref, nk_out, nv_out, nk_ref, nv_ref, head_scr, sems):
+def by_seq(scr, seqs):
+    rows = [scr[pl.ds(h, seqs, stride=8), :] for h in range(8)]
+    return jnp.concatenate(rows, axis=1).astype(jnp.bfloat16)
+
+
+def merge_last(got_ref, lam_ref, gain_ref, wo_ref, part_ref, nk_ref, nv_ref, head_scr):
     seqs = nk_ref.shape[0]
-    for h in range(8):
-        for dst, r in ((nk_ref, ROW_NKS), (nv_ref, ROW_NVS)):
-            dst[:, h * 128 : (h + 1) * 128] = jnp.concatenate(
-                [got_ref[b, r : r + 8, :].astype(jnp.float32)[h : h + 1] for b in range(seqs)], axis=0
-            ).astype(jnp.bfloat16)
-    copies = [
-        pltpu.make_async_copy(nk_ref, nk_out, sems.at[0]),
-        pltpu.make_async_copy(nv_ref, nv_out, sems.at[1]),
-    ]
-    for c in copies:
-        c.start()
+    for dst, r in ((nk_ref, ROW_NKS), (nv_ref, ROW_NVS)):
+        for b in range(seqs):
+            head_scr[b * 8 : b * 8 + 8, :] = got_ref[b, r : r + 8, :].astype(jnp.float32)
+        dst[...] = by_seq(head_scr, seqs)
     row = tails(got_ref)
     top = row(ROW_M) + row(ROW_M + 1)
     part = row(ROW_L) + row(ROW_L + 1)
@@ -215,16 +221,27 @@
         mixed = weighted(got_ref, scale, b * 16) - lam * weighted(got_ref, scale, b * 16 + 8)
         mean = jnp.mean(mixed * mixed, axis=1, keepdims=True)
         head_scr[b * 8 : b * 8 + 8, :] = mixed * lax.rsqrt(mean + EPS) * gain_ref[...]
-    heads = jnp.concatenate(
-        [head_scr[pl.ds(h, seqs, stride=8), :] for h in range(8)], axis=1
-    ).astype(jnp.bfloat16)
+    heads = by_seq(head_scr, seqs)
     part_ref[...] = lax.dot_general(
         heads, wo_ref[...], (((1,), (1,)), ((), ())), preferred_element_type=jnp.float32
     ).astype(jnp.bfloat16)
+
+
+def finish(both_ref, nk_ref, nv_ref, out, nk_out, nv_out, sum_ref, sems):
+    copies = [
+        pltpu.make_async_copy(src, dst, sems.at[i])
+        for i, (src, dst) in enumerate(((nk_ref, nk_out), (nv_ref, nv_out), (sum_ref, out)))
+    ]
+    copies[0].start()
+    copies[1].start()
+    total = both_ref[0].astype(jnp.float32) + both_ref[1].astype(jnp.float32)
+    sum_ref[...] = total.astype(sum_ref.dtype)
+    copies[2].start()
     for c in copies:
         c.wait()
 
 
+HB = pl.BlockSpec(memory_space=pltpu.HBM)
 VM = pl.BlockSpec(memory_space=pltpu.VMEM)
 SM = pl.BlockSpec(memory_space=pltpu.SMEM)
 
@@ -289,20 +306,25 @@
     row = jax.ShapeDtypeStruct((seqs, heads * width), jnp.bfloat16)
     part, new_key, new_value = pl.pallas_call(
         merge_last,
-        out_shape=(jax.ShapeDtypeStruct((seqs, w_output.shape[1]), jnp.bfloat16), row, row),
+        out_shape=(jax.ShapeDtypeStruct((seqs, w_output.shape[1]), jnp.bfloat16),) + (pltpu.VMEM(row.shape, row.dtype),) * 2,
         in_specs=[VM, SM, VM, VM],
-        out_specs=(VM, pl.BlockSpec(memory_space=pltpu.HBM), pl.BlockSpec(memory_space=pltpu.HBM)),
+        out_specs=(VM, VM, VM),
         scratch_shapes=[
-            pltpu.VMEM(row.shape, row.dtype),
-            pltpu.VMEM(row.shape, row.dtype),
             pltpu.VMEM((32, 128), jnp.float32),
-            pltpu.SemaphoreType.DMA((2,)),
         ],
         name="merge_last",
         compiler_params=pltpu.CompilerParams(vmem_limit_bytes=8 << 20),
     )(got, lam, head_gain.reshape(1, -1), w_output.T)
     both = lax.all_gather(part, "tp")
-    attended = jnp.sum(both.astype(jnp.float32), axis=0).astype(jnp.bfloat16)
+    attended, new_key, new_value = pl.pallas_call(
+        finish,
+        out_shape=(jax.ShapeDtypeStruct(part.shape, part.dtype), row, row),
+        in_specs=[VM] * 3,
+        out_specs=(HB, HB, HB),
+        scratch_shapes=[pltpu.VMEM(part.shape, part.dtype), pltpu.SemaphoreType.DMA((3,))],
+        name="finish",
+        compiler_params=pltpu.CompilerParams(vmem_limit_bytes=8 << 20),
+    )(both, new_key, new_value)
     return (attended, new_key, new_value)
 
 

time: 57.2 us -> 55.9 us (0.977)
  Pallas kernels: 6.77 us -> 6.03 us
    pallas_call x1, Pallas kernels: 3.36 us -> 2.52 us  [per_device(): pl.pallas_call(attend, out_shape=jax.ShapeDtypeStruct((lax.axis_size('kv_...]
    pallas_call x0 -> x1, Pallas kernels: none -> 0.63 us  [per_device(): pl.pallas_call(finish, out_shape=(jax.ShapeDtypeStruct(part.shape, part.d...]
    reduce_sum x1 -> x0, other arithmetic: 0.57 us -> none  [per_device(): attended = jnp.sum(both.astype(jnp.float32), axis=0).astype(jnp.bfloat16)]
where the time goes in v5:
time: 55.9 us; the launch traced here: 55.7 us
  blocking collectives  48.9 us (87%)
  Pallas kernels  6.03 us (11%)
  between operations  0.71 us (1%)
    all_to_all x3, blocking collectives, exchange(): return lax.all_to_all(array, axis, split_axis=0, concat_axis=0, tiled=True)  43.1 us
    all_gather x1, blocking collectives, per_device(): both = lax.all_gather(part, 'tp')  5.8 us
    pallas_call x1, Pallas kernels, per_device(): pl.pallas_call(attend, out_shape=jax.ShapeDtypeStruct((lax.axis_size('kv_...  2.52 us
    pallas_call x1, Pallas kernels, per_device(): pl.pallas_call(project, out_shape=jax.ShapeDtypeStruct((peers, ROWS_A, 12...  1.59 us

profile of v5, /device:TPU:1, one launch (start us, length us, event | category | flops | bytes accessed | tf_op | source)
XLA Modules:
  0.0 55.7 jit_solution(10881964551368513192)
XLA Ops:
  0.6 0.0 copy-start
  0.6 0.0 copy-start.1
  0.7 0.0 copy-start.3
  0.7 1.6 %project.1 = s16[32,40,128]{2,1,0:T(8,128)(2,1)S(1)} custom-call(bf16[4,64]{1,0:T(4,128)(2,1)} %tok_hbm.1, f32[1,64]{1,0:T(1,128)} %bitcast.11, bf16[64,1024]{1,0:T(8,128)(2,1)} %wq_hbm.1, bf16[64,1024]{1,0:T(8,128)(2,1)} %wk_hbm.1, bf16[64,1024]{1,0:T(8,128)(2,1)} %wv_hbm.1), custom_call_target="tpu_custom_call" | custom-call | flops 5000000000 | bytes 30000000 | tf_op jit(solution)/shard_map/project/pallas_call | solution.py:261
  2.3 24.8 %all_to_all.15.got_ref = s16[32,40,128]{2,1,0:T(8,128)(2,1)S(1)} all-to-all(s16[32,40,128]{2,1,0:T(8,128)(2,1)S(1)} %project.1), channel_id=1, replica_groups=mesh['dp'=4,'kv_0'=8,'kv_1'=4,'tp'=2] {'kv_0','kv_1'}, dimensions={0} | all-to-all | bytes 655360 | tf_op jit(solution)/shard_map/all_to_all | solution.py:253
  27.1 0.0 copy-done
  27.1 0.0 copy-done.1
  27.1 0.0 copy-done.3
  27.1 0.0 copy-start.2
  27.1 0.0 copy-start.4
  27.1 0.0 copy-start.5
  27.1 2.5 %attend.1 = bf16[8,72,128]{2,1,0:T(8,128)(2,1)S(1)} custom-call(s16[32,40,128]{2,1,0:T(8,128)(2,1)S(1)} %all_to_all.15.got_ref, bf16[4,4096,128]{2,1,0:T(8,128)(2,1)S(1)} %bitcast.6, bf16[4,4096,128]{2,1,0:T(8,128)(2,1)S(1)} %bitcast.7, s32[4]{0:T(128)S(1)} %copy-done.3), custom_call_target="tpu_custom_call" | custom-call | tf_op jit(solution)/shard_map/attend/pallas_call | solution.py:279
  29.6 11.0 %all_to_all.16.got_ref = bf16[8,72,128]{2,1,0:T(8,128)(2,1)S(1)} all-to-all(bf16[8,72,128]{2,1,0:T(8,128)(2,1)S(1)} %attend.1), channel_id=1, replica_groups=mesh['dp'=4,'kv_0'=8,'kv_1'=4,'tp'=2] {'kv_0'}, dimensions={0} | all-to-all | bytes 294912 | tf_op jit(solution)/shard_map/all_to_all | solution.py:253
  40.7 0.3 merge_first.1
  41.0 7.3 %all_to_all.17.got_ref = bf16[4,88,128]{2,1,0:T(8,128)(2,1)S(1)} all-to-all(bf16[4,88,128]{2,1,0:T(8,128)(2,1)S(1)} %merge_first.1), channel_id=1, replica_groups=mesh['dp'=4,'kv_0'=8,'kv_1'=4,'tp'=2] {'kv_1'}, dimensions={0} | all-to-all | bytes 180224 | tf_op jit(solution)/shard_map/all_to_all | solution.py:253
  48.2 0.0 copy-done.2
  48.2 0.0 copy-done.4
  48.2 0.0 copy-done.5
  48.3 1.0 %merge_last.1 = (bf16[4,64]{1,0:T(4,128)(2,1)S(1)}, bf16[4,1024]{1,0:T(4,128)(2,1)S(1)}, bf16[4,1024]{1,0:T(4,128)(2,1)S(1)}) custom-call(bf16[4,88,128]{2,1,0:T(8,128)(2,1)S(1)} %all_to_all.17.got_ref, f32[8]{0:T(128)S(1)} %copy-done.4, f32[1,128]{1,0:T(1,128)S(1)} %bitcast.10, bf16[64,1024]{1,0:T(8,128)(2,1)S(1)} %bitcast.8), custom_call_target="tpu_custom_call" | custom-call | tf_op jit(solution)/shard_map/merge_last/pallas_call | solution.py:307
  49.2 5.8 %all-gather.1.both_ref = bf16[2,4,64]{2,1,0:T(4,128)(2,1)S(1)} all-gather(bf16[1,4,64]{2,1,0:T(4,128)(2,1)S(1)} %bitcast.9), channel_id=2, replica_groups=mesh['dp'=4,'kv_0'=8,'kv_1'=4,'tp'=2] {'tp'}, dimensions={0}, use_global_device_ids=true | all-gather | bytes 1536 | tf_op jit(solution)/shard_map/all_gather | solution.py:318
  55.0 0.6 %finish.1 = (bf16[4,64]{1,0:T(4,128)(2,1)}, bf16[4,1024]{1,0:T(4,128)(2,1)}, bf16[4,1024]{1,0:T(4,128)(2,1)}) custom-call(bf16[2,4,64]{2,1,0:T(4,128)(2,1)S(1)} %all-gather.1.both_ref, bf16[4,1024]{1,0:T(4,128)(2,1)S(1)} %get-tuple-element.7.nk_ref, bf16[4,1024]{1,0:T(4,128)(2,1)S(1)} %get-tuple-element.8.nv_ref), custom_call_target="tpu_custom_call" | custom-call | tf_op jit(solution)/shard_map/finish/pallas_call | solution.py:319
Async XLA Ops:
  0.6 26.4 %copy-start = (bf16[4,512,8,128]{3,2,1,0:T(8,128)(2,1)S(1)}, bf16[4,512,8,128]{3,2,1,0:T(8,128)(2,1)}, u32[]{:S(2)}) copy-start(bf16[4,512,8,128]{3,2,1,0:T(8,128)(2,1)} %param.17) | copy-start | bytes 12582916
  0.6 26.4 %copy-start.1 = (bf16[4,512,8,128]{3,2,1,0:T(8,128)(2,1)S(1)}, bf16[4,512,8,128]{3,2,1,0:T(8,128)(2,1)}, u32[]{:S(2)}) copy-start(bf16[4,512,8,128]{3,2,1,0:T(8,128)(2,1)} %param.18) | copy-start | bytes 12582916
  0.7 26.4 %copy-start.3 = (s32[4]{0:T(128)S(1)}, s32[4]{0:T(128)}, u32[]{:S(2)}) copy-start(s32[4]{0:T(128)} %len_ref.1) | copy-start | bytes 52
  27.1 21.2 %copy-start.2 = (bf16[1024,64]{0,1:T(8,128)(2,1)S(1)}, bf16[1024,64]{0,1:T(8,128)(2,1)}, u32[]{:S(2)}) copy-start(bf16[1024,64]{0,1:T(8,128)(2,1)} %param.16) | copy-start | bytes 393220
  27.1 21.2 %copy-start.4 = (f32[8]{0:T(128)S(1)}, f32[8]{0:T(128)}, u32[]{:S(2)}) copy-start(f32[8]{0:T(128)} %lam_ref.1) | copy-start | bytes 100
  27.1 21.2 %copy-start.5 = (f32[128]{0:T(128)S(1)}, f32[128]{0:T(128)}, u32[]{:S(2)}) copy-start(f32[128]{0:T(128)} %param.21) | copy-start | bytes 1540

commit v6 on v5

--- a/solution.py
+++ b/solution.py
@@ -11,7 +11,7 @@
 EPS = 1e-6
 NEG = -1e30
 
-ROWS_A, BITS = 40, 14.5
+BITS = 14.5
 ROW_M, ROW_L, ROW_S, ROW_NK, ROW_NV, ROWS_C = 64, 66, 68, 70, 71, 72
 ROW_NKS, ROW_NVS, ROWS_E = 72, 80, 88
 
@@ -49,24 +49,22 @@
     whole = jnp.floor(size)
     rest = jnp.round((size - whole) * 2.0**14)
     lane = lax.broadcasted_iota(jnp.int32, (seqs, 128), 1)
+    sub = lax.broadcasted_iota(jnp.int32, (seqs, 128), 0)
     meta = jnp.where(
         lane == 0, qe, jnp.where(lane == 1, se, jnp.where(lane == 2, whole, rest))
     )
+    metas = [
+        jnp.where(lane == 4, jnp.where(sub < 2, ke[b : b + 1], ve[b : b + 1]), meta)
+        for b in range(seqs)
+    ]
     q = q.astype(jnp.int32).astype(jnp.int16)
+    kr, vr = pltpu.roll(k, 64, 1), pltpu.roll(v, 64, 1)
     for j in range(peers):
-        b = j % seqs
-        tile = jnp.concatenate(
-            [
-                k[j : j + 1],
-                v[j : j + 1],
-                jnp.broadcast_to(ke[b : b + 1], (1, 128)),
-                jnp.broadcast_to(ve[b : b + 1], (1, 128)),
-                meta,
-            ],
-            axis=0,
-        )
-        out_ref[j, 0:32, :] = q
-        out_ref[j, 32:40, :] = tile.astype(jnp.int32).astype(jnp.int16)
+        tile = jnp.concatenate([kr[j : j + 1], k[j : j + 1], vr[j : j + 1], v[j : j + 1]], axis=0)
+        tile = jnp.where(lane < 64, metas[j % seqs], tile)
+        for h in range(heads):
+            out_ref[j, h] = q[h * seqs : (h + 1) * seqs]
+        out_ref[j, heads] = tile.astype(jnp.int32).astype(jnp.int16)
 
 
 def two_pieces(a):
@@ -80,28 +78,31 @@
     width = key_ref.shape[1]
     span = width // 8
     me = lax.axis_index("kv_0") * lax.axis_size("kv_1") + lax.axis_index("kv_1")
-    total = [jnp.zeros((8, 128), jnp.float32)] * 4
-    own = jnp.zeros((8, 128), jnp.float32)
-    squares = jnp.zeros((8, 128), jnp.float32)
+    total = [jnp.zeros((seqs, 128), jnp.float32)] * 8
+    own = jnp.zeros((seqs, 128), jnp.float32)
+    squares = jnp.zeros((seqs, 128), jnp.float32)
     for j in range(peers):
-        got = got_ref[j].astype(jnp.int32).astype(jnp.float32)
-        tile = got[32:40]
+        got = [got_ref[j, i].astype(jnp.int32).astype(jnp.float32) for i in range(9)]
+        tile = got[8]
         unit = jnp.exp2(tile - BITS)
-        units = jnp.concatenate([unit[4:8, 0:1]] * 2, axis=0)
-        total = [t + got[i * 8 : i * 8 + 8] * units for i, t in enumerate(total)]
-        own = own + tile * pltpu.roll(unit, 6, 0)
+        total = [t + g * unit[:, 0:1] for t, g in zip(total, got)]
+        own = own + tile * unit[:, 4:5]
         size = tile + pltpu.roll(tile, 127, 1) * 2.0**-14
         squares = squares + size * pltpu.roll(unit, 1, 1)
+    lane1 = lax.broadcasted_iota(jnp.int32, (1, 128), 1)
+    swap = pltpu.roll(own, 64, 1)
+    own_k = jnp.where(lane1 < 64, swap[0:1], own[1:2])
+    own_v = jnp.where(lane1 < 64, swap[2:3], own[3:4])
     total = jnp.concatenate(total, axis=0)
-    inv = lax.rsqrt(jnp.broadcast_to(squares[4:8, 2:3], (4, 128)) / D + EPS)
+    inv = lax.rsqrt(jnp.broadcast_to(squares[:, 2:3], (seqs, 128)) / D + EPS)
     inv8 = jnp.concatenate([inv, inv], axis=0)
     inv32 = jnp.concatenate([inv8] * 4, axis=0)
     q = (total * inv32).astype(jnp.bfloat16).astype(jnp.float32)
     q_scr[...] = q
     seq_id = lax.broadcasted_iota(jnp.int32, (seqs, 128), 0)
     mine = jnp.sum(jnp.where(seq_id == lax.rem(me, seqs), inv, 0.0), axis=0, keepdims=True)
-    nk = (own[0:1] * mine).astype(jnp.bfloat16)
-    nv = (own[1:2] * mine).astype(jnp.bfloat16)
+    nk = (own_k * mine).astype(jnp.bfloat16)
+    nv = (own_v * mine).astype(jnp.bfloat16)
     lane = lax.broadcasted_iota(jnp.int32, (8, 128), 1)
     sub = lax.broadcasted_iota(jnp.int32, (8, 128), 0)
     lane1 = lax.broadcasted_iota(jnp.int32, (1, 128), 1)
@@ -113,6 +114,9 @@
     own_head = lax.rem(lane, 8) == sub
     col = lax.broadcasted_iota(jnp.int32, (8, width), 1)
     own_head_wide = lax.rem(col, 8) == lax.broadcasted_iota(jnp.int32, (8, width), 0)
+    col = col.astype(jnp.float32)
+    lane4 = lax.broadcasted_iota(jnp.int32, (1, seqs), 1)
+    ends = ((len_ref[...] - me * span) * 8).astype(jnp.float32)
 
     def score(b):
         qb = q_scr[pl.ds(b, 8, stride=seqs), :] * HEAD_WIDTH**-0.5
@@ -124,7 +128,7 @@
         )
 
     def weigh(b, s):
-        limit = (len_ref[b] - me * span) * 8
+        limit = jnp.sum(jnp.where(lane4 == b, ends, 0.0), axis=1, keepdims=True)
         live = jnp.logical_and(own_head_wide, col < limit)
         weights = []
         for m in range(2):
@@ -213,10 +217,9 @@
     factor = jnp.exp(top - jnp.max(top, axis=0, keepdims=True))
     total = jnp.sum(part * factor, axis=0, keepdims=True)
     scale = columns([factor / total])
-    sub = lax.broadcasted_iota(jnp.int32, (8, 128), 0)
-    lam = jnp.zeros((8, 128), jnp.float32)
-    for h in range(8):
-        lam = jnp.where(sub == h, lam_ref[h], lam)
+    lane8 = lax.broadcasted_iota(jnp.int32, (8, 8), 1)
+    sub8 = lax.broadcasted_iota(jnp.int32, (8, 8), 0)
+    lam = jnp.sum(jnp.where(lane8 == sub8, lam_ref[...], 0.0), axis=1, keepdims=True)
     for b in range(seqs):
         mixed = weighted(got_ref, scale, b * 16) - lam * weighted(got_ref, scale, b * 16 + 8)
         mean = jnp.mean(mixed * mixed, axis=1, keepdims=True)
@@ -243,7 +246,6 @@
 
 HB = pl.BlockSpec(memory_space=pltpu.HBM)
 VM = pl.BlockSpec(memory_space=pltpu.VMEM)
-SM = pl.BlockSpec(memory_space=pltpu.SMEM)
 
 
 KV = ("kv_0", "kv_1")
@@ -260,7 +262,7 @@
     seqs, span, heads, width = key_cache.shape
     sent = pl.pallas_call(
         project,
-        out_shape=jax.ShapeDtypeStruct((peers, ROWS_A, 128), jnp.int16),
+        out_shape=jax.ShapeDtypeStruct((peers, heads + 1, seqs, 128), jnp.int16),
         in_specs=[pl.BlockSpec(memory_space=pltpu.HBM)] * 5,
         out_specs=VM,
         scratch_shapes=[
@@ -279,7 +281,7 @@
     sent = pl.pallas_call(
         attend,
         out_shape=jax.ShapeDtypeStruct((lax.axis_size("kv_0"), ROWS_C, 128), jnp.bfloat16),
-        in_specs=[VM, VM, VM, SM],
+        in_specs=[VM] * 4,
         out_specs=VM,
         scratch_shapes=[
             pltpu.VMEM((32, 128), jnp.float32),
@@ -291,7 +293,7 @@
         got,
         key_cache.reshape(seqs, span * heads, width),
         value_cache.reshape(seqs, span * heads, width),
-        lengths,
+        lengths.reshape(1, -1),
     )
     got = exchange(sent, "kv_0")
     sent = pl.pallas_call(
@@ -307,14 +309,14 @@
     part, new_key, new_value = pl.pallas_call(
         merge_last,
         out_shape=(jax.ShapeDtypeStruct((seqs, w_output.shape[1]), jnp.bfloat16),) + (pltpu.VMEM(row.shape, row.dtype),) * 2,
-        in_specs=[VM, SM, VM, VM],
+        in_specs=[VM] * 4,
         out_specs=(VM, VM, VM),
         scratch_shapes=[
             pltpu.VMEM((32, 128), jnp.float32),
         ],
         name="merge_last",
         compiler_params=pltpu.CompilerParams(vmem_limit_bytes=8 << 20),
-    )(got, lam, head_gain.reshape(1, -1), w_output.T)
+    )(got, lam.reshape(1, -1), head_gain.reshape(1, -1), w_output.T)
     both = lax.all_gather(part, "tp")
     attended, new_key, new_value = pl.pallas_call(
         finish,

time: 55.9 us -> 54.1 us (0.968)
  Pallas kernels: 6.03 us -> 5.02 us
  blocking collectives: 48.9 us -> 48.2 us
    all_to_all x3, blocking collectives: 43.1 us -> 42.3 us  [exchange(): return lax.all_to_all(array, axis, split_axis=0, concat_axis=0, tiled=True)]
where the time goes in v6:
time: 54.1 us; the launch traced here: 54 us
  blocking collectives  48.2 us (89%)
  Pallas kernels  5.02 us (9%)
  between operations  0.71 us (1%)
    all_to_all x3, blocking collectives, exchange(): return lax.all_to_all(array, axis, split_axis=0, concat_axis=0, tiled=True)  42.3 us
    all_gather x1, blocking collectives, per_device(): both = lax.all_gather(part, 'tp')  5.9 us
    pallas_call x1, Pallas kernels, per_device(): pl.pallas_call(attend, out_shape=jax.ShapeDtypeStruct((lax.axis_size('kv_...  1.98 us
    pallas_call x1, Pallas kernels, per_device(): pl.pallas_call(project, out_shape=jax.ShapeDtypeStruct((peers, heads + 1,...  1.66 us

profile of v6, /device:TPU:1, one launch (start us, length us, event | category | flops | bytes accessed | tf_op | source)
XLA Modules:
  0.0 54.0 jit_solution(6938363808144357096)
XLA Ops:
  0.6 0.0 copy-start
  0.6 0.0 copy-start.1
  0.7 0.0 copy-start.3
  0.7 1.7 %project.1 = s16[32,9,4,128]{3,2,1,0:T(4,128)(2,1)S(1)} custom-call(bf16[4,64]{1,0:T(4,128)(2,1)} %tok_hbm.1, f32[1,64]{1,0:T(1,128)} %bitcast.15, bf16[64,1024]{1,0:T(8,128)(2,1)} %wq_hbm.1, bf16[64,1024]{1,0:T(8,128)(2,1)} %wk_hbm.1, bf16[64,1024]{1,0:T(8,128)(2,1)} %wv_hbm.1), custom_call_target="tpu_custom_call" | custom-call | flops 5000000000 | bytes 30000000 | tf_op jit(solution)/shard_map/project/pallas_call | solution.py:263
  2.3 24.1 %all_to_all.15.got_ref = s16[32,9,4,128]{3,2,1,0:T(4,128)(2,1)S(1)} all-to-all(s16[32,9,4,128]{3,2,1,0:T(4,128)(2,1)S(1)} %project.1), channel_id=1, replica_groups=mesh['dp'=4,'kv_0'=8,'kv_1'=4,'tp'=2] {'kv_0','kv_1'}, dimensions={0} | all-to-all | bytes 589824 | tf_op jit(solution)/shard_map/all_to_all | solution.py:255
  26.4 0.0 copy-done
  26.4 0.0 copy-done.1
  26.4 0.0 copy-done.3
  26.4 0.0 copy-start.2
  26.5 0.0 copy-start.4
  26.5 0.0 copy-start.5
  26.5 2.0 %attend.1 = bf16[8,72,128]{2,1,0:T(8,128)(2,1)S(1)} custom-call(s16[32,9,4,128]{3,2,1,0:T(4,128)(2,1)S(1)} %all_to_all.15.got_ref, bf16[4,4096,128]{2,1,0:T(8,128)(2,1)S(1)} %bitcast.8, bf16[4,4096,128]{2,1,0:T(8,128)(2,1)S(1)} %bitcast.9, s32[1,4]{1,0:T(1,128)S(1)} %bitcast.12), custom_call_target="tpu_custom_call" | custom-call | tf_op jit(solution)/shard_map/attend/pallas_call | solution.py:281
  28.5 11.1 %all_to_all.16.got_ref = bf16[8,72,128]{2,1,0:T(8,128)(2,1)S(1)} all-to-all(bf16[8,72,128]{2,1,0:T(8,128)(2,1)S(1)} %attend.1), channel_id=1, replica_groups=mesh['dp'=4,'kv_0'=8,'kv_1'=4,'tp'=2] {'kv_0'}, dimensions={0} | all-to-all | bytes 294912 | tf_op jit(solution)/shard_map/all_to_all | solution.py:255
  39.5 0.3 merge_first.1
  39.8 7.1 %all_to_all.17.got_ref = bf16[4,88,128]{2,1,0:T(8,128)(2,1)S(1)} all-to-all(bf16[4,88,128]{2,1,0:T(8,128)(2,1)S(1)} %merge_first.1), channel_id=1, replica_groups=mesh['dp'=4,'kv_0'=8,'kv_1'=4,'tp'=2] {'kv_1'}, dimensions={0} | all-to-all | bytes 180224 | tf_op jit(solution)/shard_map/all_to_all | solution.py:255
  47.0 0.0 copy-done.2
  47.0 0.0 copy-done.4
  47.0 0.0 copy-done.5
  47.0 0.4 merge_last.1
  47.4 5.9 %all-gather.1.both_ref = bf16[2,4,64]{2,1,0:T(4,128)(2,1)S(1)} all-gather(bf16[1,4,64]{2,1,0:T(4,128)(2,1)S(1)} %bitcast.11), channel_id=2, replica_groups=mesh['dp'=4,'kv_0'=8,'kv_1'=4,'tp'=2] {'tp'}, dimensions={0}, use_global_device_ids=true | all-gather | bytes 1536 | tf_op jit(solution)/shard_map/all_gather | solution.py:320
  53.3 0.6 %finish.1 = (bf16[4,64]{1,0:T(4,128)(2,1)}, bf16[4,1024]{1,0:T(4,128)(2,1)}, bf16[4,1024]{1,0:T(4,128)(2,1)}) custom-call(bf16[2,4,64]{2,1,0:T(4,128)(2,1)S(1)} %all-gather.1.both_ref, bf16[4,1024]{1,0:T(4,128)(2,1)S(1)} %get-tuple-element.7.nk_ref, bf16[4,1024]{1,0:T(4,128)(2,1)S(1)} %get-tuple-element.8.nv_ref), custom_call_target="tpu_custom_call" | custom-call | tf_op jit(solution)/shard_map/finish/pallas_call | solution.py:321
Async XLA Ops:
  0.6 25.8 %copy-start = (bf16[4,512,8,128]{3,2,1,0:T(8,128)(2,1)S(1)}, bf16[4,512,8,128]{3,2,1,0:T(8,128)(2,1)}, u32[]{:S(2)}) copy-start(bf16[4,512,8,128]{3,2,1,0:T(8,128)(2,1)} %param.17) | copy-start | bytes 12582916
  0.6 25.8 %copy-start.1 = (bf16[4,512,8,128]{3,2,1,0:T(8,128)(2,1)S(1)}, bf16[4,512,8,128]{3,2,1,0:T(8,128)(2,1)}, u32[]{:S(2)}) copy-start(bf16[4,512,8,128]{3,2,1,0:T(8,128)(2,1)} %param.18) | copy-start | bytes 12582916
  0.7 25.8 %copy-start.3 = (s32[4]{0:T(128)S(1)}, s32[4]{0:T(128)}, u32[]{:S(2)}) copy-start(s32[4]{0:T(128)} %param.19) | copy-start | bytes 52
  26.4 20.5 %copy-start.2 = (bf16[1024,64]{0,1:T(8,128)(2,1)S(1)}, bf16[1024,64]{0,1:T(8,128)(2,1)}, u32[]{:S(2)}) copy-start(bf16[1024,64]{0,1:T(8,128)(2,1)} %param.16) | copy-start | bytes 393220
  26.5 20.5 %copy-start.4 = (f32[8]{0:T(128)S(1)}, f32[8]{0:T(128)}, u32[]{:S(2)}) copy-start(f32[8]{0:T(128)} %param.20) | copy-start | bytes 100
  26.5 20.5 %copy-start.5 = (f32[128]{0:T(128)S(1)}, f32[128]{0:T(128)}, u32[]{:S(2)}) copy-start(f32[128]{0:T(128)} %param.21) | copy-start | bytes 1540

commit v7 on v6

--- a/solution.py
+++ b/solution.py
@@ -230,14 +230,14 @@
     ).astype(jnp.bfloat16)
 
 
-def finish(both_ref, nk_ref, nv_ref, out, nk_out, nv_out, sum_ref, sems):
+def finish(part_ref, other_ref, nk_ref, nv_ref, out, nk_out, nv_out, sum_ref, sems):
     copies = [
         pltpu.make_async_copy(src, dst, sems.at[i])
         for i, (src, dst) in enumerate(((nk_ref, nk_out), (nv_ref, nv_out), (sum_ref, out)))
     ]
     copies[0].start()
     copies[1].start()
-    total = both_ref[0].astype(jnp.float32) + both_ref[1].astype(jnp.float32)
+    total = part_ref[...].astype(jnp.float32) + other_ref[...].astype(jnp.float32)
     sum_ref[...] = total.astype(sum_ref.dtype)
     copies[2].start()
     for c in copies:
@@ -317,16 +317,16 @@
         name="merge_last",
         compiler_params=pltpu.CompilerParams(vmem_limit_bytes=8 << 20),
     )(got, lam.reshape(1, -1), head_gain.reshape(1, -1), w_output.T)
-    both = lax.all_gather(part, "tp")
+    other = lax.ppermute(part, "tp", [(0, 1), (1, 0)])
     attended, new_key, new_value = pl.pallas_call(
         finish,
         out_shape=(jax.ShapeDtypeStruct(part.shape, part.dtype), row, row),
-        in_specs=[VM] * 3,
+        in_specs=[VM] * 4,
         out_specs=(HB, HB, HB),
         scratch_shapes=[pltpu.VMEM(part.shape, part.dtype), pltpu.SemaphoreType.DMA((3,))],
         name="finish",
         compiler_params=pltpu.CompilerParams(vmem_limit_bytes=8 << 20),
-    )(both, new_key, new_value)
+    )(part, other, new_key, new_value)
     return (attended, new_key, new_value)
 
 

time: 54.1 us -> 53.5 us (0.989)
  blocking collectives: 48.2 us -> 42.3 us
  starting transfers between devices: 0 us -> 4.45 us
  waiting for transfers between devices: 0 us -> 0.82 us
    all_gather x1 -> x0, blocking collectives: 5.9 us -> none  [per_device(): both = lax.all_gather(part, 'tp')]
    ppermute x0 -> x1, starting transfers between devices: none -> 4.45 us  [per_device(): other = lax.ppermute(part, 'tp', [(0, 1), (1, 0)])]
    ppermute x0 -> x1, waiting for transfers between devices: none -> 0.82 us  [per_device(): other = lax.ppermute(part, 'tp', [(0, 1), (1, 0)])]
  transfers between devices with their start and end apart: 0 -> 1, of which waited for: 0 -> 1; matrix products, arithmetic and copies ran while one was open for 0% -> 0% of each run, Pallas kernels for 0% -> 0%
where the time goes in v7:
time: 53.5 us; the launch traced here: 53.3 us
  blocking collectives  42.3 us (79%)
  Pallas kernels  5.02 us (9%)
  starting transfers between devices  4.45 us (8%)
  waiting for transfers between devices  0.82 us (2%)
  between operations  0.71 us (1%)
    all_to_all x3, blocking collectives, exchange(): return lax.all_to_all(array, axis, split_axis=0, concat_axis=0, tiled=True)  42.3 us
    ppermute x1, starting transfers between devices, per_device(): other = lax.ppermute(part, 'tp', [(0, 1), (1, 0)])  4.45 us
    pallas_call x1, Pallas kernels, per_device(): pl.pallas_call(attend, out_shape=jax.ShapeDtypeStruct((lax.axis_size('kv_...  1.98 us
    pallas_call x1, Pallas kernels, per_device(): pl.pallas_call(project, out_shape=jax.ShapeDtypeStruct((peers, heads + 1,...  1.66 us
  transfers between devices with their start and end apart: 1, of which 1 were waited for; matrix products, arithmetic and copies ran while one was open for 0% of the time, Pallas kernels for 0%

profile of v7, /device:TPU:1, one launch (start us, length us, event | category | flops | bytes accessed | tf_op | source)
XLA Modules:
  0.0 53.3 jit_solution(6398695376582076965)
XLA Ops:
  0.6 0.0 copy-start
  0.6 0.0 copy-start.1
  0.7 0.0 copy-start.3
  0.7 1.7 %project.1 = s16[32,9,4,128]{3,2,1,0:T(4,128)(2,1)S(1)} custom-call(bf16[4,64]{1,0:T(4,128)(2,1)} %tok_hbm.1, f32[1,64]{1,0:T(1,128)} %bitcast.13, bf16[64,1024]{1,0:T(8,128)(2,1)} %wq_hbm.1, bf16[64,1024]{1,0:T(8,128)(2,1)} %wk_hbm.1, bf16[64,1024]{1,0:T(8,128)(2,1)} %wv_hbm.1), custom_call_target="tpu_custom_call" | custom-call | flops 5000000000 | bytes 30000000 | tf_op jit(solution)/shard_map/project/pallas_call | solution.py:263
  2.3 24.1 %all_to_all.15.got_ref = s16[32,9,4,128]{3,2,1,0:T(4,128)(2,1)S(1)} all-to-all(s16[32,9,4,128]{3,2,1,0:T(4,128)(2,1)S(1)} %project.1), channel_id=1, replica_groups=mesh['dp'=4,'kv_0'=8,'kv_1'=4,'tp'=2] {'kv_0','kv_1'}, dimensions={0} | all-to-all | bytes 589824 | tf_op jit(solution)/shard_map/all_to_all | solution.py:255
  26.4 0.0 copy-done
  26.4 0.0 copy-done.1
  26.4 0.0 copy-done.3
  26.4 0.0 copy-start.2
  26.5 0.0 copy-start.4
  26.5 0.0 copy-start.5
  26.5 2.0 %attend.1 = bf16[8,72,128]{2,1,0:T(8,128)(2,1)S(1)} custom-call(s16[32,9,4,128]{3,2,1,0:T(4,128)(2,1)S(1)} %all_to_all.15.got_ref, bf16[4,4096,128]{2,1,0:T(8,128)(2,1)S(1)} %bitcast.7, bf16[4,4096,128]{2,1,0:T(8,128)(2,1)S(1)} %bitcast.8, s32[1,4]{1,0:T(1,128)S(1)} %bitcast.10), custom_call_target="tpu_custom_call" | custom-call | tf_op jit(solution)/shard_map/attend/pallas_call | solution.py:281
  28.5 11.1 %all_to_all.16.got_ref = bf16[8,72,128]{2,1,0:T(8,128)(2,1)S(1)} all-to-all(bf16[8,72,128]{2,1,0:T(8,128)(2,1)S(1)} %attend.1), channel_id=1, replica_groups=mesh['dp'=4,'kv_0'=8,'kv_1'=4,'tp'=2] {'kv_0'}, dimensions={0} | all-to-all | bytes 294912 | tf_op jit(solution)/shard_map/all_to_all | solution.py:255
  39.5 0.3 merge_first.1
  39.8 7.1 %all_to_all.17.got_ref = bf16[4,88,128]{2,1,0:T(8,128)(2,1)S(1)} all-to-all(bf16[4,88,128]{2,1,0:T(8,128)(2,1)S(1)} %merge_first.1), channel_id=1, replica_groups=mesh['dp'=4,'kv_0'=8,'kv_1'=4,'tp'=2] {'kv_1'}, dimensions={0} | all-to-all | bytes 180224 | tf_op jit(solution)/shard_map/all_to_all | solution.py:255
  47.0 0.0 copy-done.2
  47.0 0.0 copy-done.4
  47.0 0.0 copy-done.5
  47.0 0.4 merge_last.1
  47.4 4.4 %collective-permute-start = (bf16[4,64]{1,0:T(4,128)(2,1)S(1)}, bf16[4,64]{1,0:T(4,128)(2,1)S(1)}, u32[]{:S(2)}, u32[]{:S(2)}) collective-permute-start(bf16[4,64]{1,0:T(4,128)(2,1)S(1)} %get-tuple-element.6.part_ref), channel_id=1, source_target_pairs={{0,1},{1,0},{2,3},{3,2},{4,5},{5,4},{6,7},{7,6},{8,9},{9,8},{10,11... | collective-permute-start | bytes 1544 | tf_op jit(solution)/shard_map/ppermute | solution.py:320
  51.9 0.8 %collective-permute-done.other_ref = bf16[4,64]{1,0:T(4,128)(2,1)S(1)} collective-permute-done((bf16[4,64]{1,0:T(4,128)(2,1)S(1)}, bf16[4,64]{1,0:T(4,128)(2,1)S(1)}, u32[]{:S(2)}, u32[]{:S(2)}) %collective-permute-start) | collective-permute-done | bytes 544 | tf_op jit(solution)/shard_map/ppermute | solution.py:320
  52.7 0.6 %finish.1 = (bf16[4,64]{1,0:T(4,128)(2,1)}, bf16[4,1024]{1,0:T(4,128)(2,1)}, bf16[4,1024]{1,0:T(4,128)(2,1)}) custom-call(bf16[4,64]{1,0:T(4,128)(2,1)S(1)} %get-tuple-element.6.part_ref, bf16[4,64]{1,0:T(4,128)(2,1)S(1)} %collective-permute-done.other_ref, bf16[4,1024]{1,0:T(4,128)(2,1)S(1)} %get-tuple-element.7.nk_ref, ...), custom_call_target="tpu_custom_call" | custom-call | tf_op jit(solution)/shard_map/finish/pallas_call | solution.py:321
Async XLA Ops:
  0.6 25.8 %copy-start = (bf16[4,512,8,128]{3,2,1,0:T(8,128)(2,1)S(1)}, bf16[4,512,8,128]{3,2,1,0:T(8,128)(2,1)}, u32[]{:S(2)}) copy-start(bf16[4,512,8,128]{3,2,1,0:T(8,128)(2,1)} %param.17) | copy-start | bytes 12582916
  0.6 25.8 %copy-start.1 = (bf16[4,512,8,128]{3,2,1,0:T(8,128)(2,1)S(1)}, bf16[4,512,8,128]{3,2,1,0:T(8,128)(2,1)}, u32[]{:S(2)}) copy-start(bf16[4,512,8,128]{3,2,1,0:T(8,128)(2,1)} %param.18) | copy-start | bytes 12582916
  0.7 25.8 %copy-start.3 = (s32[4]{0:T(128)S(1)}, s32[4]{0:T(128)}, u32[]{:S(2)}) copy-start(s32[4]{0:T(128)} %param.19) | copy-start | bytes 52
  26.4 20.5 %copy-start.2 = (bf16[1024,64]{0,1:T(8,128)(2,1)S(1)}, bf16[1024,64]{0,1:T(8,128)(2,1)}, u32[]{:S(2)}) copy-start(bf16[1024,64]{0,1:T(8,128)(2,1)} %param.16) | copy-start | bytes 393220
  26.5 20.5 %copy-start.4 = (f32[8]{0:T(128)S(1)}, f32[8]{0:T(128)}, u32[]{:S(2)}) copy-start(f32[8]{0:T(128)} %param.20) | copy-start | bytes 100
  26.5 20.5 %copy-start.5 = (f32[128]{0:T(128)S(1)}, f32[128]{0:T(128)}, u32[]{:S(2)}) copy-start(f32[128]{0:T(128)} %param.21) | copy-start | bytes 1540
  47.4 5.3 %collective-permute-start = (bf16[4,64]{1,0:T(4,128)(2,1)S(1)}, bf16[4,64]{1,0:T(4,128)(2,1)S(1)}, u32[]{:S(2)}, u32[]{:S(2)}) collective-permute-start(bf16[4,64]{1,0:T(4,128)(2,1)S(1)} %get-tuple-element.6.part_ref), channel_id=1, source_target_pairs={{0,1},{1,0},{2,3},{3,2},{4,5},{5,4},{6,7},{7,6},{8,9},{9,8},{10,11... | collective-permute-start | bytes 1544 | tf_op jit(solution)/shard_map/ppermute | solution.py:320

commit v8 on v7

--- a/solution.py
+++ b/solution.py
@@ -59,12 +59,13 @@
     ]
     q = q.astype(jnp.int32).astype(jnp.int16)
     kr, vr = pltpu.roll(k, 64, 1), pltpu.roll(v, 64, 1)
-    for j in range(peers):
+    for i in range(peers):
+        j = i % 8 * seqs + i // 8
         tile = jnp.concatenate([kr[j : j + 1], k[j : j + 1], vr[j : j + 1], v[j : j + 1]], axis=0)
         tile = jnp.where(lane < 64, metas[j % seqs], tile)
         for h in range(heads):
-            out_ref[j, h] = q[h * seqs : (h + 1) * seqs]
-        out_ref[j, heads] = tile.astype(jnp.int32).astype(jnp.int16)
+            out_ref[i, h] = q[h * seqs : (h + 1) * seqs]
+        out_ref[i, heads] = tile.astype(jnp.int32).astype(jnp.int16)
 
 
 def two_pieces(a):
@@ -78,17 +79,24 @@
     width = key_ref.shape[1]
     span = width // 8
     me = lax.axis_index("kv_0") * lax.axis_size("kv_1") + lax.axis_index("kv_1")
-    total = [jnp.zeros((seqs, 128), jnp.float32)] * 8
-    own = jnp.zeros((seqs, 128), jnp.float32)
-    squares = jnp.zeros((seqs, 128), jnp.float32)
-    for j in range(peers):
-        got = [got_ref[j, i].astype(jnp.int32).astype(jnp.float32) for i in range(9)]
+    total = [jnp.zeros((8, 128), jnp.float32)] * 8
+    own = jnp.zeros((8, 128), jnp.float32)
+    squares = jnp.zeros((8, 128), jnp.float32)
+    for j in range(0, peers, 2):
+        got = [
+            jnp.concatenate([got_ref[j, i].astype(jnp.int32), got_ref[j + 1, i].astype(jnp.int32)], axis=0)
+            for i in range(9)
+        ]
+        got = [g.astype(jnp.float32) for g in got]
         tile = got[8]
         unit = jnp.exp2(tile - BITS)
         total = [t + g * unit[:, 0:1] for t, g in zip(total, got)]
         own = own + tile * unit[:, 4:5]
         size = tile + pltpu.roll(tile, 127, 1) * 2.0**-14
         squares = squares + size * pltpu.roll(unit, 1, 1)
+    total = [t[:seqs] + t[seqs:] for t in total]
+    own = own[:seqs] + own[seqs:]
+    squares = squares[:seqs] + squares[seqs:]
     lane1 = lax.broadcasted_iota(jnp.int32, (1, 128), 1)
     swap = pltpu.roll(own, 64, 1)
     own_k = jnp.where(lane1 < 64, swap[0:1], own[1:2])
@@ -274,10 +282,19 @@
             pltpu.SemaphoreType.DMA((5,)),
         ],
         name="project",
-        cost_estimate=pl.CostEstimate(flops=5_000_000_000, bytes_accessed=30_000_000, transcendentals=0),
         compiler_params=pltpu.CompilerParams(vmem_limit_bytes=8 << 20),
     )(*(pltpu.with_memory_space_constraint(a, pltpu.HBM) for a in (tokens, norm_gain.reshape(1, -1), w_query, w_key, w_value)))
-    got = exchange(sent, KV)
+    sent = pl.pallas_call(
+        lambda given, same: None,
+        out_shape=jax.ShapeDtypeStruct(sent.shape, sent.dtype),
+        in_specs=[pl.BlockSpec(memory_space=pl.ANY)],
+        out_specs=pl.BlockSpec(memory_space=pl.ANY),
+        input_output_aliases={0: 0},
+        name="hold",
+        cost_estimate=pl.CostEstimate(flops=5_000_000_000, bytes_accessed=30_000_000, transcendentals=0),
+        compiler_params=pltpu.CompilerParams(vmem_limit_bytes=1 << 20),
+    )(sent)
+    got = exchange(sent, KV[::-1])
     sent = pl.pallas_call(
         attend,
         out_shape=jax.ShapeDtypeStruct((lax.axis_size("kv_0"), ROWS_C, 128), jnp.bfloat16),

time: 53.5 us -> 53.3 us (level)
  no operation moved by 1% of the time
where the time goes in v8:
time: 53.3 us; the launch traced here: 53.1 us
  blocking collectives  42.3 us (79%)
  Pallas kernels  4.83 us (9%)
  starting transfers between devices  4.36 us (8%)
  waiting for transfers between devices  0.82 us (2%)
  between operations  0.72 us (1%)
    all_to_all x3, blocking collectives, exchange(): return lax.all_to_all(array, axis, split_axis=0, concat_axis=0, tiled=True)  42.3 us
    ppermute x1, starting transfers between devices, per_device(): other = lax.ppermute(part, 'tp', [(0, 1), (1, 0)])  4.36 us
    pallas_call x1, Pallas kernels, per_device(): pl.pallas_call(attend, out_shape=jax.ShapeDtypeStruct((lax.axis_size('kv_...  1.94 us
    pallas_call x1, Pallas kernels, per_device(): pl.pallas_call(project, out_shape=jax.ShapeDtypeStruct((peers, heads + 1,...  1.51 us
  transfers between devices with their start and end apart: 1, of which 1 were waited for; matrix products, arithmetic and copies ran while one was open for 0% of the time, Pallas kernels for 0%

profile of v8, /device:TPU:1, one launch (start us, length us, event | category | flops | bytes accessed | tf_op | source)
XLA Modules:
  0.0 53.1 jit_solution(1990317370868355178)
XLA Ops:
  0.6 1.5 %project.1.given = s16[32,9,4,128]{3,2,1,0:T(4,128)(2,1)S(1)} custom-call(bf16[4,64]{1,0:T(4,128)(2,1)} %tok_hbm.1, f32[1,64]{1,0:T(1,128)} %bitcast.13, bf16[64,1024]{1,0:T(8,128)(2,1)} %wq_hbm.1, bf16[64,1024]{1,0:T(8,128)(2,1)} %wk_hbm.1, bf16[64,1024]{1,0:T(8,128)(2,1)} %wv_hbm.1), custom_call_target="tpu_custom_call" | custom-call | tf_op jit(solution)/shard_map/project/pallas_call | solution.py:271
  2.1 0.0 copy-start
  2.2 0.0 copy-start.1
  2.2 0.0 copy-start.3
  2.2 22.0 %all_to_all.15.got_ref = s16[32,9,4,128]{3,2,1,0:T(4,128)(2,1)S(1)} all-to-all(s16[32,9,4,128]{3,2,1,0:T(4,128)(2,1)S(1)} %hold.1), channel_id=1, replica_groups=mesh['dp'=4,'kv_0'=8,'kv_1'=4,'tp'=2] {'kv_1','kv_0'}, dimensions={0} | all-to-all | bytes 589824 | tf_op jit(solution)/shard_map/all_to_all | solution.py:263
  24.2 0.0 copy-done
  24.2 0.0 copy-done.1
  24.2 0.0 copy-done.3
  24.2 0.0 copy-start.2
  24.2 0.0 copy-start.4
  24.2 0.0 copy-start.5
  24.3 1.9 %attend.1 = bf16[8,72,128]{2,1,0:T(8,128)(2,1)S(1)} custom-call(s16[32,9,4,128]{3,2,1,0:T(4,128)(2,1)S(1)} %all_to_all.15.got_ref, bf16[4,4096,128]{2,1,0:T(8,128)(2,1)S(1)} %bitcast.7, bf16[4,4096,128]{2,1,0:T(8,128)(2,1)S(1)} %bitcast.8, s32[1,4]{1,0:T(1,128)S(1)} %bitcast.10), custom_call_target="tpu_custom_call" | custom-call | tf_op jit(solution)/shard_map/attend/pallas_call | solution.py:298
  26.2 12.9 %all_to_all.16.got_ref = bf16[8,72,128]{2,1,0:T(8,128)(2,1)S(1)} all-to-all(bf16[8,72,128]{2,1,0:T(8,128)(2,1)S(1)} %attend.1), channel_id=1, replica_groups=mesh['dp'=4,'kv_0'=8,'kv_1'=4,'tp'=2] {'kv_0'}, dimensions={0} | all-to-all | bytes 294912 | tf_op jit(solution)/shard_map/all_to_all | solution.py:263
  39.1 0.3 merge_first.1
  39.5 7.4 %all_to_all.17.got_ref = bf16[4,88,128]{2,1,0:T(8,128)(2,1)S(1)} all-to-all(bf16[4,88,128]{2,1,0:T(8,128)(2,1)S(1)} %merge_first.1), channel_id=1, replica_groups=mesh['dp'=4,'kv_0'=8,'kv_1'=4,'tp'=2] {'kv_1'}, dimensions={0} | all-to-all | bytes 180224 | tf_op jit(solution)/shard_map/all_to_all | solution.py:263
  46.8 0.0 copy-done.2
  46.8 0.0 copy-done.4
  46.8 0.0 copy-done.5
  46.8 0.4 merge_last.1
  47.3 4.4 %collective-permute-start = (bf16[4,64]{1,0:T(4,128)(2,1)S(1)}, bf16[4,64]{1,0:T(4,128)(2,1)S(1)}, u32[]{:S(2)}, u32[]{:S(2)}) collective-permute-start(bf16[4,64]{1,0:T(4,128)(2,1)S(1)} %get-tuple-element.6.part_ref), channel_id=1, source_target_pairs={{0,1},{1,0},{2,3},{3,2},{4,5},{5,4},{6,7},{7,6},{8,9},{9,8},{10,11... | collective-permute-start | bytes 1544 | tf_op jit(solution)/shard_map/ppermute | solution.py:337
  51.6 0.8 %collective-permute-done.other_ref = bf16[4,64]{1,0:T(4,128)(2,1)S(1)} collective-permute-done((bf16[4,64]{1,0:T(4,128)(2,1)S(1)}, bf16[4,64]{1,0:T(4,128)(2,1)S(1)}, u32[]{:S(2)}, u32[]{:S(2)}) %collective-permute-start) | collective-permute-done | bytes 544 | tf_op jit(solution)/shard_map/ppermute | solution.py:337
  52.4 0.6 %finish.1 = (bf16[4,64]{1,0:T(4,128)(2,1)}, bf16[4,1024]{1,0:T(4,128)(2,1)}, bf16[4,1024]{1,0:T(4,128)(2,1)}) custom-call(bf16[4,64]{1,0:T(4,128)(2,1)S(1)} %get-tuple-element.6.part_ref, bf16[4,64]{1,0:T(4,128)(2,1)S(1)} %collective-permute-done.other_ref, bf16[4,1024]{1,0:T(4,128)(2,1)S(1)} %get-tuple-element.7.nk_ref, ...), custom_call_target="tpu_custom_call" | custom-call | tf_op jit(solution)/shard_map/finish/pallas_call | solution.py:338
  (1 shorter events, 0.0 us)
Async XLA Ops:
  2.1 22.1 %copy-start = (bf16[4,512,8,128]{3,2,1,0:T(8,128)(2,1)S(1)}, bf16[4,512,8,128]{3,2,1,0:T(8,128)(2,1)}, u32[]{:S(2)}) copy-start(bf16[4,512,8,128]{3,2,1,0:T(8,128)(2,1)} %param.17) | copy-start | bytes 12582916
  2.2 22.1 %copy-start.1 = (bf16[4,512,8,128]{3,2,1,0:T(8,128)(2,1)S(1)}, bf16[4,512,8,128]{3,2,1,0:T(8,128)(2,1)}, u32[]{:S(2)}) copy-start(bf16[4,512,8,128]{3,2,1,0:T(8,128)(2,1)} %param.18) | copy-start | bytes 12582916
  2.2 22.0 %copy-start.3 = (s32[4]{0:T(128)S(1)}, s32[4]{0:T(128)}, u32[]{:S(2)}) copy-start(s32[4]{0:T(128)} %param.19) | copy-start | bytes 52
  24.2 22.6 %copy-start.2 = (bf16[1024,64]{0,1:T(8,128)(2,1)S(1)}, bf16[1024,64]{0,1:T(8,128)(2,1)}, u32[]{:S(2)}) copy-start(bf16[1024,64]{0,1:T(8,128)(2,1)} %param.16) | copy-start | bytes 393220
  24.2 22.6 %copy-start.4 = (f32[8]{0:T(128)S(1)}, f32[8]{0:T(128)}, u32[]{:S(2)}) copy-start(f32[8]{0:T(128)} %param.20) | copy-start | bytes 100
  24.2 22.6 %copy-start.5 = (f32[128]{0:T(128)S(1)}, f32[128]{0:T(128)}, u32[]{:S(2)}) copy-start(f32[128]{0:T(128)} %param.21) | copy-start | bytes 1540
  47.3 5.2 %collective-permute-start = (bf16[4,64]{1,0:T(4,128)(2,1)S(1)}, bf16[4,64]{1,0:T(4,128)(2,1)S(1)}, u32[]{:S(2)}, u32[]{:S(2)}) collective-permute-start(bf16[4,64]{1,0:T(4,128)(2,1)S(1)} %get-tuple-element.6.part_ref), channel_id=1, source_target_pairs={{0,1},{1,0},{2,3},{3,2},{4,5},{5,4},{6,7},{7,6},{8,9},{9,8},{10,11... | collective-permute-start | bytes 1544 | tf_op jit(solution)/shard_map/ppermute | solution.py:337

commit v9 on v8

--- a/solution.py
+++ b/solution.py
@@ -213,12 +213,8 @@
     return jnp.concatenate(rows, axis=1).astype(jnp.bfloat16)
 
 
-def merge_last(got_ref, lam_ref, gain_ref, wo_ref, part_ref, nk_ref, nv_ref, head_scr):
-    seqs = nk_ref.shape[0]
-    for dst, r in ((nk_ref, ROW_NKS), (nv_ref, ROW_NVS)):
-        for b in range(seqs):
-            head_scr[b * 8 : b * 8 + 8, :] = got_ref[b, r : r + 8, :].astype(jnp.float32)
-        dst[...] = by_seq(head_scr, seqs)
+def merge_last(got_ref, lam_ref, gain_ref, wo_ref, part_ref, head_scr):
+    seqs = part_ref.shape[0]
     row = tails(got_ref)
     top = row(ROW_M) + row(ROW_M + 1)
     part = row(ROW_L) + row(ROW_L + 1)
@@ -238,18 +234,22 @@
     ).astype(jnp.bfloat16)
 
 
-def finish(part_ref, other_ref, nk_ref, nv_ref, out, nk_out, nv_out, sum_ref, sems):
-    copies = [
-        pltpu.make_async_copy(src, dst, sems.at[i])
-        for i, (src, dst) in enumerate(((nk_ref, nk_out), (nv_ref, nv_out), (sum_ref, out)))
-    ]
-    copies[0].start()
-    copies[1].start()
-    total = part_ref[...].astype(jnp.float32) + other_ref[...].astype(jnp.float32)
-    sum_ref[...] = total.astype(sum_ref.dtype)
-    copies[2].start()
+def emit(got_ref, nk_out, nv_out, nk_ref, nv_ref, scr, sems):
+    seqs = nk_ref.shape[0]
+    copies = []
+    for i, (out, dst, r) in enumerate(((nk_out, nk_ref, ROW_NKS), (nv_out, nv_ref, ROW_NVS))):
+        for b in range(seqs):
+            scr[b * 8 : b * 8 + 8, :] = got_ref[b, r : r + 8, :].astype(jnp.float32)
+        dst[...] = by_seq(scr, seqs)
+        copies.append(pltpu.make_async_copy(dst, out, sems.at[i]))
+        copies[i].start()
     for c in copies:
         c.wait()
+
+
+def finish(part_ref, other_ref, out_ref):
+    total = part_ref[...].astype(jnp.float32) + other_ref[...].astype(jnp.float32)
+    out_ref[...] = total.astype(out_ref.dtype)
 
 
 HB = pl.BlockSpec(memory_space=pltpu.HBM)
@@ -323,27 +323,39 @@
     )(got)
     got = exchange(sent, "kv_1")
     row = jax.ShapeDtypeStruct((seqs, heads * width), jnp.bfloat16)
-    part, new_key, new_value = pl.pallas_call(
+    part = pl.pallas_call(
         merge_last,
-        out_shape=(jax.ShapeDtypeStruct((seqs, w_output.shape[1]), jnp.bfloat16),) + (pltpu.VMEM(row.shape, row.dtype),) * 2,
+        out_shape=jax.ShapeDtypeStruct((seqs, w_output.shape[1]), jnp.bfloat16),
         in_specs=[VM] * 4,
-        out_specs=(VM, VM, VM),
-        scratch_shapes=[
-            pltpu.VMEM((32, 128), jnp.float32),
-        ],
+        out_specs=VM,
+        scratch_shapes=[pltpu.VMEM((32, 128), jnp.float32)],
         name="merge_last",
         compiler_params=pltpu.CompilerParams(vmem_limit_bytes=8 << 20),
     )(got, lam.reshape(1, -1), head_gain.reshape(1, -1), w_output.T)
     other = lax.ppermute(part, "tp", [(0, 1), (1, 0)])
-    attended, new_key, new_value = pl.pallas_call(
+    new_key, new_value = pl.pallas_call(
+        emit,
+        out_shape=(row, row),
+        in_specs=[VM],
+        out_specs=(HB, HB),
+        scratch_shapes=[
+            pltpu.VMEM(row.shape, row.dtype),
+            pltpu.VMEM(row.shape, row.dtype),
+            pltpu.VMEM((32, 128), jnp.float32),
+            pltpu.SemaphoreType.DMA((2,)),
+        ],
+        name="emit",
+        cost_estimate=pl.CostEstimate(flops=1_000_000, bytes_accessed=1_000_000, transcendentals=0),
+        compiler_params=pltpu.CompilerParams(vmem_limit_bytes=8 << 20),
+    )(got)
+    attended = pl.pallas_call(
         finish,
-        out_shape=(jax.ShapeDtypeStruct(part.shape, part.dtype), row, row),
-        in_specs=[VM] * 4,
-        out_specs=(HB, HB, HB),
-        scratch_shapes=[pltpu.VMEM(part.shape, part.dtype), pltpu.SemaphoreType.DMA((3,))],
+        out_shape=jax.ShapeDtypeStruct(part.shape, part.dtype),
+        in_specs=[VM] * 2,
+        out_specs=VM,
         name="finish",
         compiler_params=pltpu.CompilerParams(vmem_limit_bytes=8 << 20),
-    )(part, other, new_key, new_value)
+    )(part, other)
     return (attended, new_key, new_value)
 
 

time: 53.3 us -> 53.2 us (level)
  waiting for transfers between devices: 0.82 us -> 0.18 us
  Pallas kernels: 4.83 us -> 5.4 us
    ppermute x1, waiting for transfers between devices: 0.82 us -> 0.18 us  [per_device(): other = lax.ppermute(part, 'tp', [(0, 1), (1, 0)])]
    pallas_call x2 -> x3, Pallas kernels: 1.07 us -> 1.65 us  [the longest x1 0.64 us: per_device(): pl.pallas_call(emit, out_shape=(row, row), in_specs=[VM], out_specs=(HB,...]
  transfers between devices with their start and end apart: 1 -> 1, of which waited for: 1 -> 1; matrix products, arithmetic and copies ran while one was open for 0% -> 0% of each run, Pallas kernels for 0% -> 1%
where the time goes in v9:
time: 53.2 us; the launch traced here: 53 us
  blocking collectives  42.3 us (80%)
  Pallas kernels  5.4 us (10%)
  starting transfers between devices  4.36 us (8%)
  between operations  0.72 us (1%)
    all_to_all x3, blocking collectives, exchange(): return lax.all_to_all(array, axis, split_axis=0, concat_axis=0, tiled=True)  42.3 us
    ppermute x1, starting transfers between devices, per_device(): other = lax.ppermute(part, 'tp', [(0, 1), (1, 0)])  4.36 us
    pallas_call x1, Pallas kernels, per_device(): pl.pallas_call(attend, out_shape=jax.ShapeDtypeStruct((lax.axis_size('kv_...  1.94 us
    pallas_call x1, Pallas kernels, per_device(): pl.pallas_call(project, out_shape=jax.ShapeDtypeStruct((peers, heads + 1,...  1.51 us
  transfers between devices with their start and end apart: 1, of which 1 were waited for; matrix products, arithmetic and copies ran while one was open for 0% of the time, Pallas kernels for 1%

profile of v9, /device:TPU:1, one launch (start us, length us, event | category | flops | bytes accessed | tf_op | source)
XLA Modules:
  0.0 53.0 jit_solution(17470240560058162487)
XLA Ops:
  0.6 1.5 %project.1.given = s16[32,9,4,128]{3,2,1,0:T(4,128)(2,1)S(1)} custom-call(bf16[4,64]{1,0:T(4,128)(2,1)} %tok_hbm.1, f32[1,64]{1,0:T(1,128)} %bitcast.13, bf16[64,1024]{1,0:T(8,128)(2,1)} %wq_hbm.1, bf16[64,1024]{1,0:T(8,128)(2,1)} %wk_hbm.1, bf16[64,1024]{1,0:T(8,128)(2,1)} %wv_hbm.1), custom_call_target="tpu_custom_call" | custom-call | tf_op jit(solution)/shard_map/project/pallas_call | solution.py:271
  2.1 0.0 copy-start
  2.2 0.0 copy-start.1
  2.2 0.0 copy-start.3
  2.2 22.0 %all_to_all.15.got_ref = s16[32,9,4,128]{3,2,1,0:T(4,128)(2,1)S(1)} all-to-all(s16[32,9,4,128]{3,2,1,0:T(4,128)(2,1)S(1)} %hold.1), channel_id=1, replica_groups=mesh['dp'=4,'kv_0'=8,'kv_1'=4,'tp'=2] {'kv_1','kv_0'}, dimensions={0} | all-to-all | bytes 589824 | tf_op jit(solution)/shard_map/all_to_all | solution.py:263
  24.2 0.0 copy-done
  24.2 0.0 copy-done.1
  24.2 0.0 copy-done.3
  24.2 0.0 copy-start.2
  24.2 0.0 copy-start.4
  24.2 0.0 copy-start.5
  24.3 1.9 %attend.1 = bf16[8,72,128]{2,1,0:T(8,128)(2,1)S(1)} custom-call(s16[32,9,4,128]{3,2,1,0:T(4,128)(2,1)S(1)} %all_to_all.15.got_ref, bf16[4,4096,128]{2,1,0:T(8,128)(2,1)S(1)} %bitcast.7, bf16[4,4096,128]{2,1,0:T(8,128)(2,1)S(1)} %bitcast.8, s32[1,4]{1,0:T(1,128)S(1)} %bitcast.10), custom_call_target="tpu_custom_call" | custom-call | tf_op jit(solution)/shard_map/attend/pallas_call | solution.py:298
  26.2 12.9 %all_to_all.16.got_ref = bf16[8,72,128]{2,1,0:T(8,128)(2,1)S(1)} all-to-all(bf16[8,72,128]{2,1,0:T(8,128)(2,1)S(1)} %attend.1), channel_id=1, replica_groups=mesh['dp'=4,'kv_0'=8,'kv_1'=4,'tp'=2] {'kv_0'}, dimensions={0} | all-to-all | bytes 294912 | tf_op jit(solution)/shard_map/all_to_all | solution.py:263
  39.1 0.3 merge_first.1
  39.5 7.4 %all_to_all.17.got_ref = bf16[4,88,128]{2,1,0:T(8,128)(2,1)S(1)} all-to-all(bf16[4,88,128]{2,1,0:T(8,128)(2,1)S(1)} %merge_first.1), channel_id=1, replica_groups=mesh['dp'=4,'kv_0'=8,'kv_1'=4,'tp'=2] {'kv_1'}, dimensions={0} | all-to-all | bytes 180224 | tf_op jit(solution)/shard_map/all_to_all | solution.py:263
  46.8 0.0 copy-done.2
  46.8 0.0 copy-done.4
  46.8 0.0 copy-done.5
  46.8 0.4 merge_last.1.part_ref
  47.3 4.4 %collective-permute-start = (bf16[4,64]{1,0:T(4,128)(2,1)S(1)}, bf16[4,64]{1,0:T(4,128)(2,1)S(1)}, u32[]{:S(2)}, u32[]{:S(2)}) collective-permute-start(bf16[4,64]{1,0:T(4,128)(2,1)S(1)} %merge_last.1.part_ref), channel_id=1, source_target_pairs={{0,1},{1,0},{2,3},{3,2},{4,5},{5,4},{6,7},{7,6},{8,9},{9,8},{10,11... | collective-permute-start | bytes 1544 | tf_op jit(solution)/shard_map/ppermute | solution.py:335
  51.6 0.6 %emit.1 = (bf16[4,1024]{1,0:T(4,128)(2,1)}, bf16[4,1024]{1,0:T(4,128)(2,1)}) custom-call(bf16[4,88,128]{2,1,0:T(8,128)(2,1)S(1)} %all_to_all.17.got_ref), custom_call_target="tpu_custom_call" | custom-call | flops 1000000 | bytes 1000000 | tf_op jit(solution)/shard_map/emit/pallas_call | solution.py:336
  52.3 0.2 collective-permute-done.other_ref
  52.4 0.6 %finish.1 = bf16[4,64]{1,0:T(4,128)(2,1)} custom-call(bf16[4,64]{1,0:T(4,128)(2,1)S(1)} %merge_last.1.part_ref, bf16[4,64]{1,0:T(4,128)(2,1)S(1)} %collective-permute-done.other_ref), custom_call_target="tpu_custom_call" | custom-call | tf_op jit(solution)/shard_map/finish/pallas_call | solution.py:351
  (1 shorter events, 0.0 us)
Async XLA Ops:
  2.1 22.1 %copy-start = (bf16[4,512,8,128]{3,2,1,0:T(8,128)(2,1)S(1)}, bf16[4,512,8,128]{3,2,1,0:T(8,128)(2,1)}, u32[]{:S(2)}) copy-start(bf16[4,512,8,128]{3,2,1,0:T(8,128)(2,1)} %param.17) | copy-start | bytes 12582916
  2.2 22.1 %copy-start.1 = (bf16[4,512,8,128]{3,2,1,0:T(8,128)(2,1)S(1)}, bf16[4,512,8,128]{3,2,1,0:T(8,128)(2,1)}, u32[]{:S(2)}) copy-start(bf16[4,512,8,128]{3,2,1,0:T(8,128)(2,1)} %param.18) | copy-start | bytes 12582916
  2.2 22.0 %copy-start.3 = (s32[4]{0:T(128)S(1)}, s32[4]{0:T(128)}, u32[]{:S(2)}) copy-start(s32[4]{0:T(128)} %param.19) | copy-start | bytes 52
  24.2 22.6 %copy-start.2 = (bf16[1024,64]{0,1:T(8,128)(2,1)S(1)}, bf16[1024,64]{0,1:T(8,128)(2,1)}, u32[]{:S(2)}) copy-start(bf16[1024,64]{0,1:T(8,128)(2,1)} %param.16) | copy-start | bytes 393220
  24.2 22.6 %copy-start.4 = (f32[8]{0:T(128)S(1)}, f32[8]{0:T(128)}, u32[]{:S(2)}) copy-start(f32[8]{0:T(128)} %param.20) | copy-start | bytes 100
  24.2 22.6 %copy-start.5 = (f32[128]{0:T(128)S(1)}, f32[128]{0:T(128)}, u32[]{:S(2)}) copy-start(f32[128]{0:T(128)} %param.21) | copy-start | bytes 1540
  47.3 5.2 %collective-permute-start = (bf16[4,64]{1,0:T(4,128)(2,1)S(1)}, bf16[4,64]{1,0:T(4,128)(2,1)S(1)}, u32[]{:S(2)}, u32[]{:S(2)}) collective-permute-start(bf16[4,64]{1,0:T(4,128)(2,1)S(1)} %merge_last.1.part_ref), channel_id=1, source_target_pairs={{0,1},{1,0},{2,3},{3,2},{4,5},{5,4},{6,7},{7,6},{8,9},{9,8},{10,11... | collective-permute-start | bytes 1544 | tf_op jit(solution)/shard_map/ppermute | solution.py:335
